TPU v7x, 32 devices: a whole 2x2x4 slice. The times are simulated.
32 devices in a mesh: tp: 32 (over z, y, x, core).
Axes of the slice: x: 2, y: 2, z: 4, core: 2. Of those that a mesh axis runs over, the one named last changes fastest.
Arguments:
- tokens: bfloat16 [32, 8, 4096], P('tp'), may hold values from -6 to 6
- block_norm_gain: float32 [2, 4096], replicated, may hold values from 0.1 to 1.9
- receptance_weight: bfloat16 [2, 32, 4096, 64], P(None, 'tp'), may hold values from -0.09375 to 0.09375
- key_weight: bfloat16 [2, 32, 4096, 64], P(None, 'tp'), may hold values from -0.09375 to 0.09375
- value_weight: bfloat16 [2, 32, 4096, 64], P(None, 'tp'), may hold values from -0.09375 to 0.09375
- decay_weight: bfloat16 [2, 32, 4096, 64], P(None, 'tp'), may hold values from -0.09375 to 0.09375
- learning_rate_weight: bfloat16 [2, 32, 4096, 64], P(None, 'tp'), may hold values from -0.09375 to 0.09375
- gate_weight: bfloat16 [2, 32, 4096, 64], P(None, 'tp'), may hold values from -0.09375 to 0.09375
- decay_bias_fixed: float32 [2, 2048], replicated, may hold values from -5 to 2
- self_token_weight: float32 [2, 2048], replicated, may hold values from -1.5 to 1.5
- readout_norm_gain: float32 [2, 2048], replicated, may hold values from 0.1 to 1.9
- output_weight: bfloat16 [2, 32, 64, 4096], P(None, 'tp'), may hold values from -0.125 to 0.125
- state: float32 [2, 32, 256, 4096], P(None, 'tp'), may hold values from -3 to 3
Outputs:
- mixed: bfloat16 [32, 8, 4096], P('tp')
- new_state: float32 [2, 32, 256, 4096], P(None, 'tp')
All inputs are finite; a program needn't handle non-finite values.
Results may differ from a plain program's by a relative error of at most 0.018.
Values may be sent and summed in bfloat16 or wider, within the bound.
A program may use at most 128 MiB of HBM per device.

v0:
```python
import jax
import jax.numpy as jnp
from jax import lax
from jax.sharding import PartitionSpec as P

D = 4096


RMS_EPS = 1e-06
GROUP_EPS = 0.00064


def swapped(shard, axis, stride):
    return lax.ppermute(shard, axis, [(i, i ^ 1 << stride) for i in range(lax.axis_size(axis))])


def for_sending(shard):

    def short(part):
        return part.astype(jnp.bfloat16) if part.dtype == jnp.float32 else part

    return jax.tree.map(short, shard)


def recurrent_update(
    layer_state,
    receptance_vector,
    key_vector,
    value_vector,
    decay_logits,
    learning_rate_logits,
    gate_logits,
    decay_constant,
    self_term_scale,
    head_gain_slice,
):
    highest = lax.Precision.HIGHEST
    shrink = jnp.exp(-jnp.exp(-jax.nn.softplus(-(decay_constant + decay_logits)) - 0.5))
    rate = jax.nn.sigmoid(learning_rate_logits)
    normed = key_vector * lax.rsqrt(jnp.sum(key_vector * key_vector, -1, keepdims=True) + 1.0)
    removed = jnp.einsum("...ij,...j->...i", layer_state, normed, precision=highest)
    layer_state = (
        layer_state * shrink[..., None, :]
        - removed[..., :, None] * (normed * rate)[..., None, :]
        + value_vector[..., :, None] * (key_vector * rate)[..., None, :]
    )
    readout = jnp.einsum("...ij,...j->...i", layer_state, receptance_vector, precision=highest)
    center = jnp.mean(readout, -1, keepdims=True)
    spread = jnp.mean(jnp.square(readout - center), -1, keepdims=True)
    normed_output = (readout - center) * lax.rsqrt(spread + GROUP_EPS) * head_gain_slice
    self_term = (
        jnp.sum(receptance_vector * key_vector * self_term_scale, -1, keepdims=True) * value_vector
    )
    return (
        ((normed_output + self_term) * jax.nn.sigmoid(gate_logits)).astype(jnp.bfloat16),
        layer_state,
    )


def double_gather(piece, position, first_bit, count, mover):
    for offset in range(count):
        which_bit = first_bit + offset
        partner = mover(piece, which_bit)
        lower_self = position >> which_bit & 1 == 0
        piece = jnp.where(
            lower_self, jnp.concatenate([piece, partner], 0), jnp.concatenate([partner, piece], 0)
        )
    return piece


def halve_sum(members, position, first_bit, count, mover):
    for offset in reversed(range(count)):
        which_bit = first_bit + offset
        upper_self = position >> which_bit & 1 == 1
        sends = tuple(
            (
                jnp.where(
                    upper_self, member[: member.shape[0] // 2], member[member.shape[0] // 2 :]
                )
                for member in members
            )
        )
        keeps = tuple(
            (
                jnp.where(
                    upper_self, member[member.shape[0] // 2 :], member[: member.shape[0] // 2]
                )
                for member in members
            )
        )
        arrived = mover(sends, which_bit)
        members = tuple((kept + got for kept, got in zip(keeps, arrived)))
    return members


def on_device(
    tokens,
    block_norm_gain,
    receptance_weight,
    key_weight,
    value_weight,
    decay_weight,
    learning_rate_weight,
    gate_weight,
    decay_bias_fixed,
    self_token_weight,
    readout_norm_gain,
    output_weight,
    state,
):
    columns_dev = tokens.shape[2]
    row_blocks = D // columns_dev
    low_bits = row_blocks.bit_length() - 1
    head_count = lax.axis_size("tp") // row_blocks
    high_bits = head_count.bit_length() - 1
    position = lax.axis_index("tp")
    head_index = position // row_blocks
    row_block = position % row_blocks
    head_size = receptance_weight.shape[3]
    seq_tile = tokens.shape[1]
    move_rows = lambda payload, which_bit: swapped(payload, "tp", which_bit)
    move_proj = lambda payload, which_bit: swapped(payload, "tp", which_bit)
    move_outs = lambda payload, which_bit: jax.tree.map(
        lambda part, own: part.astype(own.dtype),
        swapped(for_sending(payload), "tp", which_bit),
        payload,
    )
    move_split = lambda payload, which_bit: jax.tree.map(
        lambda part, own: part.astype(own.dtype),
        swapped(for_sending(payload), "tp", which_bit),
        payload,
    )

    def mixer(columns, layer_index):
        gain_cols = lax.dynamic_slice_in_dim(
            block_norm_gain[layer_index], row_block * columns_dev, columns_dev
        )
        wide = columns.astype(jnp.float32)
        scaled = (wide * gain_cols).astype(jnp.bfloat16)
        squares = jnp.sum(wide * wide, axis=1)
        weights = jnp.concatenate(
            [
                receptance_weight[layer_index, 0],
                key_weight[layer_index, 0],
                value_weight[layer_index, 0],
                decay_weight[layer_index, 0],
                learning_rate_weight[layer_index, 0],
                gate_weight[layer_index, 0],
            ],
            axis=1,
        )
        partial_value = jnp.dot(scaled, weights, preferred_element_type=jnp.float32)
        summed, total_sq = halve_sum((partial_value, squares), position, 0, low_bits, move_proj)
        projected = summed * lax.rsqrt(total_sq / D + RMS_EPS)[:, None]
        output_pieces = jnp.split(projected, 6, axis=1)

        def head_columns(table):
            return lax.dynamic_slice_in_dim(table[layer_index], head_index * head_size, head_size)

        layer_state = state[layer_index, 0].reshape(-1, head_size, head_size)
        out_tile, layer_state = recurrent_update(
            layer_state,
            *output_pieces,
            head_columns(decay_bias_fixed),
            head_columns(self_token_weight),
            head_columns(readout_norm_gain)
        )
        out_all = double_gather(out_tile, position, 0, low_bits, move_outs)
        branch = jnp.dot(out_all, output_weight[layer_index, 0], preferred_element_type=jnp.float32)
        return (branch, layer_state.reshape(layer_state.shape[0], head_size * head_size))

    columns = double_gather(tokens[0], position, low_bits, high_bits, move_rows)
    first_branch, first_memory = mixer(columns, 0)
    (tile_sum,) = halve_sum((first_branch,), position, low_bits, high_bits, move_split)
    tile_one = (tokens[0].astype(jnp.float32) + tile_sum).astype(jnp.bfloat16)
    columns = double_gather(tile_one, position, low_bits, high_bits, move_rows)
    second_branch, second_memory = mixer(columns, 1)
    (tile_sum,) = halve_sum((second_branch,), position, low_bits, high_bits, move_split)
    resid_rows = lax.dynamic_slice_in_dim(columns, head_index * seq_tile, seq_tile, 0)
    mixed = (resid_rows.astype(jnp.float32) + tile_sum).astype(jnp.bfloat16)
    new_state = jnp.stack([first_memory, second_memory])[:, None]
    return (mixed[None], new_state)


def solution(mesh):
    return jax.shard_map(
        on_device,
        mesh=mesh,
        in_specs=(
            P("tp", None, None),
            P(),
            P(None, "tp", None, None),
            P(None, "tp", None, None),
            P(None, "tp", None, None),
            P(None, "tp", None, None),
            P(None, "tp", None, None),
            P(None, "tp", None, None),
            P(),
            P(),
            P(),
            P(None, "tp", None, None),
            P(None, "tp", None, None),
        ),
        out_specs=(P("tp", None, None), P(None, "tp", None, None)),
        check_vma=False,
    )
```

profile of v0, /device:TPU:0, one launch (start us, length us, event | category | flops | bytes accessed | tf_op | source)
XLA Modules:
  0.0 353.4 jit_solution(11987146937723311241)
XLA Ops:
  1.2 1.3 bitcast_dynamic-update-slice_fusion.11
  2.5 8.0 %fusion.76 = (f32[1,1,256,4096]{3,2,1,0:T(8,128)}, f32[1,1,256,4096]{3,2,1,0:T(8,128)}) fusion(f32[2,1,256,4096]{3,2,1,0:T(8,128)} %param.25), kind=kLoop, calls=%fused_computation.161 | loop fusion | bytes 16777216 | tf_op jit(solution)/shard_map/slice | solution.py:160
  10.7 0.9 copy-done.9
  12.1 1.7 copy-done.15
  13.8 1.7 copy-done.16
  15.6 2.6 collective-permute-start.1
  18.7 3.5 %collective-permute-done.1 = bf16[16,4096]{1,0:T(8,128)(2,1)S(1)} collective-permute-done((bf16[16,4096]{1,0:T(8,128)(2,1)S(1)}, bf16[16,4096]{1,0:T(8,128)(2,1)S(1)}, u32[]{:S(2)}, u32[]{:S(2)}) %collective-permute-start.1) | collective-permute-done | bytes 131104 | tf_op jit(solution)/shard_map/ppermute | solution.py:14
  22.3 1.8 collective-permute-start.2
  24.8 5.8 %collective-permute-done.2 = bf16[32,4096]{1,0:T(8,128)(2,1)S(1)} collective-permute-done((bf16[32,4096]{1,0:T(8,128)(2,1)S(1)}, bf16[32,4096]{1,0:T(8,128)(2,1)S(1)}, u32[]{:S(2)}, u32[]{:S(2)}) %collective-permute-start.2) | collective-permute-done | bytes 262176 | tf_op jit(solution)/shard_map/ppermute | solution.py:14
  30.6 1.6 collective-permute-start.3
  32.9 10.7 %collective-permute-done.3 = bf16[64,4096]{1,0:T(8,128)(2,1)S(1)} collective-permute-done((bf16[64,4096]{1,0:T(8,128)(2,1)S(1)}, bf16[64,4096]{1,0:T(8,128)(2,1)S(1)}, u32[]{:S(2)}, u32[]{:S(2)}) %collective-permute-start.3) | collective-permute-done | bytes 524320 | tf_op jit(solution)/shard_map/ppermute | solution.py:14
  43.8 2.3 collective-permute-start.4
  46.1 5.7 %copy.53 = f32[1,1,256,4096]{2,3,1,0:T(8,128)} copy(f32[1,1,256,4096]{3,2,1,0:T(8,128)} %get-tuple-element.17) | data formatting | bytes 8388608
  52.4 1.0 bitcast_dynamic-update-slice_fusion.6
  53.5 37.0 %collective-permute-done.4 = bf16[128,4096]{1,0:T(8,128)(2,1)S(1)} collective-permute-done((bf16[128,4096]{1,0:T(8,128)(2,1)S(1)}, bf16[128,4096]{1,0:T(8,128)(2,1)S(1)}, u32[]{:S(2)}, u32[]{:S(2)}) %collective-permute-start.4) | collective-permute-done | bytes 1048608 | tf_op jit(solution)/shard_map/ppermute | solution.py:14
  91.2 3.1 fusion.10
  95.3 1.5 multiply_reduce_fusion.2
  97.7 2.0 copy-done.5
  100.0 48.0 %collective-permute-done.5 = bf16[128,4096]{1,0:T(8,128)(2,1)S(1)} collective-permute-done((bf16[128,4096]{1,0:T(8,128)(2,1)S(1)}, bf16[128,4096]{1,0:T(8,128)(2,1)S(1)}, u32[]{:S(2)}, u32[]{:S(2)}) %collective-permute-start.5) | collective-permute-done | bytes 1048608 | tf_op jit(solution)/shard_map/ppermute | solution.py:14
  148.0 2.5 convert_add_fusion.1
  150.7 13.3 %collective-permute-done.6 = bf16[64,4096]{1,0:T(8,128)(2,1)} collective-permute-done((bf16[64,4096]{1,0:T(8,128)(2,1)S(1)}, bf16[64,4096]{1,0:T(8,128)(2,1)}, u32[]{:S(2)}, u32[]{:S(2)}) %collective-permute-start.6) | collective-permute-done | bytes 524320 | tf_op jit(solution)/shard_map/ppermute | solution.py:14
  163.9 1.2 convert_add_fusion.3
  165.2 6.7 %collective-permute-done.7 = bf16[32,4096]{1,0:T(8,128)(2,1)S(1)} collective-permute-done((bf16[32,4096]{1,0:T(8,128)(2,1)S(1)}, bf16[32,4096]{1,0:T(8,128)(2,1)S(1)}, u32[]{:S(2)}, u32[]{:S(2)}) %collective-permute-start.7) | collective-permute-done | bytes 262176 | tf_op jit(solution)/shard_map/ppermute | solution.py:14
  172.1 5.0 %collective-permute-done.8 = bf16[16,4096]{1,0:T(8,128)(2,1)S(1)} collective-permute-done((bf16[16,4096]{1,0:T(8,128)(2,1)S(1)}, bf16[16,4096]{1,0:T(8,128)(2,1)S(1)}, u32[]{:S(2)}, u32[]{:S(2)}) %collective-permute-start.8) | collective-permute-done | bytes 131104 | tf_op jit(solution)/shard_map/ppermute | solution.py:14
  177.2 1.2 collective-permute-done.9
  178.7 1.1 collective-permute-done.10
  179.9 5.5 %collective-permute-done.11 = bf16[16,4096]{1,0:T(8,128)(2,1)S(1)} collective-permute-done((bf16[16,4096]{1,0:T(8,128)(2,1)S(1)}, bf16[16,4096]{1,0:T(8,128)(2,1)S(1)}, u32[]{:S(2)}, u32[]{:S(2)}) %collective-permute-start.11) | collective-permute-done | bytes 131104 | tf_op jit(solution)/shard_map/ppermute | solution.py:14
  185.9 7.2 %collective-permute-done.12 = bf16[32,4096]{1,0:T(8,128)(2,1)S(1)} collective-permute-done((bf16[32,4096]{1,0:T(8,128)(2,1)S(1)}, bf16[32,4096]{1,0:T(8,128)(2,1)S(1)}, u32[]{:S(2)}, u32[]{:S(2)}) %collective-permute-start.12) | collective-permute-done | bytes 262176 | tf_op jit(solution)/shard_map/ppermute | solution.py:14
  193.8 11.7 %collective-permute-done.13 = bf16[64,4096]{1,0:T(8,128)(2,1)S(1)} collective-permute-done((bf16[64,4096]{1,0:T(8,128)(2,1)S(1)}, bf16[64,4096]{1,0:T(8,128)(2,1)S(1)}, u32[]{:S(2)}, u32[]{:S(2)}) %collective-permute-start.13) | collective-permute-done | bytes 524320 | tf_op jit(solution)/shard_map/ppermute | solution.py:14
  205.7 1.7 collective-permute-start.14
  207.4 5.7 %copy.54 = f32[1,1,256,4096]{2,3,1,0:T(8,128)} copy(f32[1,1,256,4096]{3,2,1,0:T(8,128)} %get-tuple-element.16) | data formatting | bytes 8388608
  214.8 37.0 %collective-permute-done.14 = bf16[128,4096]{1,0:T(8,128)(2,1)S(1)} collective-permute-done((bf16[128,4096]{1,0:T(8,128)(2,1)S(1)}, bf16[128,4096]{1,0:T(8,128)(2,1)S(1)}, u32[]{:S(2)}, u32[]{:S(2)}) %collective-permute-start.14) | collective-permute-done | bytes 1048608 | tf_op jit(solution)/shard_map/ppermute | solution.py:14
  251.8 1.2 fusion.3
  253.0 1.4 copy-done.6
  254.4 1.0 fusion.13
  256.6 1.6 multiply_reduce_fusion
  259.2 2.0 copy-done.4
  261.4 48.3 %collective-permute-done.15 = bf16[128,4096]{1,0:T(8,128)(2,1)S(1)} collective-permute-done((bf16[128,4096]{1,0:T(8,128)(2,1)S(1)}, bf16[128,4096]{1,0:T(8,128)(2,1)S(1)}, u32[]{:S(2)}, u32[]{:S(2)}) %collective-permute-start.15) | collective-permute-done | bytes 1048608 | tf_op jit(solution)/shard_map/ppermute | solution.py:14
  309.8 2.5 convert_add_fusion
  313.6 1.0 copy-done.1
  314.6 1.4 bitcast_add_fusion.1
  316.0 10.3 %collective-permute-done.16 = bf16[64,4096]{1,0:T(8,128)(2,1)S(1)} collective-permute-done((bf16[64,4096]{1,0:T(8,128)(2,1)S(1)}, bf16[64,4096]{1,0:T(8,128)(2,1)S(1)}, u32[]{:S(2)}, u32[]{:S(2)}) %collective-permute-start.16) | collective-permute-done | bytes 524320 | tf_op jit(solution)/shard_map/ppermute | solution.py:14
  327.5 6.5 %collective-permute-done.17 = bf16[32,4096]{1,0:T(8,128)(2,1)S(1)} collective-permute-done((bf16[32,4096]{1,0:T(8,128)(2,1)S(1)}, bf16[32,4096]{1,0:T(8,128)(2,1)S(1)}, u32[]{:S(2)}, u32[]{:S(2)}) %collective-permute-start.17) | collective-permute-done | bytes 262176 | tf_op jit(solution)/shard_map/ppermute | solution.py:14
  335.0 1.4 bitcast_add_fusion
  336.4 2.7 collective-permute-done.18
  339.3 3.8 %maximum_bitcast_fusion = f32[2,1,256,4096]{2,3,0,1:T(8,128)} fusion(f32[1,256,4096]{1,2,0:T(8,128)S(1)} %bitcast_add_fusion, f32[1,256,4096]{1,2,0:T(8,128)S(1)} %bitcast_add_fusion.1), kind=kLoop, calls=%fused_computation | loop fusion | flops 2097152 | bytes 16777216 | tf_op jit(solution)/shard_map/broadcast_in_dim | solution.py:181
  343.0 8.9 %copy.30 = f32[2,1,256,4096]{3,2,1,0:T(8,128)} copy(f32[2,1,256,4096]{2,3,0,1:T(8,128)} %maximum_bitcast_fusion) | data formatting | bytes 16777216
  351.9 1.5 fusion.22
  (117 shorter events, 16.6 us)
Async XLA Ops:
  0.6 14.9 %collective-permute-start = (bf16[8,4096]{1,0:T(8,128)(2,1)}, bf16[8,4096]{1,0:T(8,128)(2,1)S(1)}, u32[]{:S(2)}, u32[]{:S(2)}) collective-permute-start(bf16[8,4096]{1,0:T(8,128)(2,1)} %bitcast.90), channel_id=1, source_target_pairs={{0,1},{1,0},{2,3},{3,2},{4,5},{5,4},{6,7},{7,6},{8,9},{9,8},{10,11... | collective-permute-start | bytes 196616 | tf_op jit(solution)/shard_map/ppermute | solution.py:14
  2.5 8.0 %copy-start.7 = (bf16[2,1,4096,64]{2,3,1,0:T(8,128)(2,1)S(1)}, bf16[2,1,4096,64]{2,3,1,0:T(8,128)(2,1)}, u32[]{:S(2)}) copy-start(bf16[2,1,4096,64]{2,3,1,0:T(8,128)(2,1)} %param.16) | copy-start | bytes 3145732
  2.5 8.1 %copy-start.8 = (bf16[2,1,4096,64]{2,3,1,0:T(8,128)(2,1)S(1)}, bf16[2,1,4096,64]{2,3,1,0:T(8,128)(2,1)}, u32[]{:S(2)}) copy-start(bf16[2,1,4096,64]{2,3,1,0:T(8,128)(2,1)} %param.17) | copy-start | bytes 3145732
  10.4 1.2 copy-start.9
  10.4 1.5 copy-start.10
  10.5 3.3 copy-start.18
  10.5 5.1 %copy-start.14 = (bf16[1,8,4096]{2,1,0:T(8,128)(2,1)S(1)}, bf16[1,8,4096]{2,1,0:T(8,128)(2,1)}, u32[]{:S(2)}) copy-start(bf16[1,8,4096]{2,1,0:T(8,128)(2,1)} %param.13) | copy-start | bytes 196612
  10.5 7.6 %copy-start.19 = (f32[2,2048]{1,0:T(2,128)S(1)}, f32[2,2048]{1,0:T(2,128)}, u32[]{:S(2)}) copy-start(f32[2,2048]{1,0:T(2,128)} %param.22) | copy-start | bytes 49156
  10.5 13.7 %copy-start.20 = (f32[2,2048]{1,0:T(2,128)S(1)}, f32[2,2048]{1,0:T(2,128)}, u32[]{:S(2)}) copy-start(f32[2,2048]{1,0:T(2,128)} %param.21) | copy-start | bytes 49156
  10.6 21.7 %copy-start.21 = (f32[2,2048]{1,0:T(2,128)S(1)}, f32[2,2048]{1,0:T(2,128)}, u32[]{:S(2)}) copy-start(f32[2,2048]{1,0:T(2,128)} %param.23) | copy-start | bytes 49156
  12.1 1.7 copy-start.15
  13.8 1.7 copy-start.16
  15.6 6.7 %collective-permute-start.1 = (bf16[16,4096]{1,0:T(8,128)(2,1)S(1)}, bf16[16,4096]{1,0:T(8,128)(2,1)S(1)}, u32[]{:S(2)}, u32[]{:S(2)}) collective-permute-start(bf16[16,4096]{1,0:T(8,128)(2,1)S(1)} %maximum_select_fusion.9), channel_id=1, source_target_pairs={{0,2},{1,3},{2,0},{3,1},{4,6},{5,7},{6,4},{7,5},{8,10},{9,11},{10,... | collective-permute-start | bytes 393224 | tf_op jit(solution)/shard_map/ppermute | solution.py:14
  22.3 8.2 %collective-permute-start.2 = (bf16[32,4096]{1,0:T(8,128)(2,1)S(1)}, bf16[32,4096]{1,0:T(8,128)(2,1)S(1)}, u32[]{:S(2)}, u32[]{:S(2)}) collective-permute-start(bf16[32,4096]{1,0:T(8,128)(2,1)S(1)} %maximum_select_fusion.7), channel_id=1, source_target_pairs={{0,4},{1,5},{2,6},{3,7},{4,0},{5,1},{6,2},{7,3},{8,12},{9,13},{10,... | collective-permute-start | bytes 786440 | tf_op jit(solution)/shard_map/ppermute | solution.py:14
  30.6 13.0 %collective-permute-start.3 = (bf16[64,4096]{1,0:T(8,128)(2,1)S(1)}, bf16[64,4096]{1,0:T(8,128)(2,1)S(1)}, u32[]{:S(2)}, u32[]{:S(2)}) collective-permute-start(bf16[64,4096]{1,0:T(8,128)(2,1)S(1)} %maximum_select_fusion.4), channel_id=1, source_target_pairs={{0,8},{1,9},{2,10},{3,11},{4,12},{5,13},{6,14},{7,15},{8,0},{9,1},... | collective-permute-start | bytes 1572872 | tf_op jit(solution)/shard_map/ppermute | solution.py:14
  43.8 46.7 %collective-permute-start.4 = (bf16[128,4096]{1,0:T(8,128)(2,1)S(1)}, bf16[128,4096]{1,0:T(8,128)(2,1)S(1)}, u32[]{:S(2)}, u32[]{:S(2)}) collective-permute-start(bf16[128,4096]{1,0:T(8,128)(2,1)S(1)} %maximum_select_fusion.2), channel_id=1, source_target_pairs={{0,16},{1,17},{2,18},{3,19},{4,20},{5,21},{6,22},{7,23},{8,24},{9,... | collective-permute-start | bytes 3145736 | tf_op jit(solution)/shard_map/ppermute | solution.py:14
  46.1 6.3 %copy-start.11 = (bf16[2,1,4096,64]{2,3,1,0:T(8,128)(2,1)S(1)}, bf16[2,1,4096,64]{2,3,1,0:T(8,128)(2,1)}, u32[]{:S(2)}) copy-start(bf16[2,1,4096,64]{2,3,1,0:T(8,128)(2,1)} %param.20) | copy-start | bytes 3145732
  91.2 3.4 copy-start
  94.6 2.2 copy-start.12
  94.6 2.2 copy-start.22
  97.7 2.0 copy-start.5
  99.9 48.1 %collective-permute-start.5 = (bf16[128,4096]{1,0:T(8,128)(2,1)S(1)}, bf16[128,4096]{1,0:T(8,128)(2,1)S(1)}, u32[]{:S(2)}, u32[]{:S(2)}) collective-permute-start(bf16[128,4096]{1,0:T(8,128)(2,1)S(1)} %select_convert_fusion.1), channel_id=1, source_target_pairs={{0,16},{1,17},{2,18},{3,19},{4,20},{5,21},{6,22},{7,23},{8,24},{9,... | collective-permute-start | bytes 3145736 | tf_op jit(solution)/shard_map/ppermute | solution.py:14
  150.6 13.3 %collective-permute-start.6 = (bf16[64,4096]{1,0:T(8,128)(2,1)S(1)}, bf16[64,4096]{1,0:T(8,128)(2,1)}, u32[]{:S(2)}, u32[]{:S(2)}) collective-permute-start(bf16[64,4096]{1,0:T(8,128)(2,1)S(1)} %select_convert_fusion.3), channel_id=1, source_target_pairs={{0,8},{1,9},{2,10},{3,11},{4,12},{5,13},{6,14},{7,15},{8,0},{9,1},... | collective-permute-start | bytes 1572872 | tf_op jit(solution)/shard_map/ppermute | solution.py:14
  165.2 6.8 %collective-permute-start.7 = (bf16[32,4096]{1,0:T(8,128)(2,1)S(1)}, bf16[32,4096]{1,0:T(8,128)(2,1)S(1)}, u32[]{:S(2)}, u32[]{:S(2)}) collective-permute-start(bf16[32,4096]{1,0:T(8,128)(2,1)S(1)} %select_convert_fusion.5), channel_id=1, source_target_pairs={{0,4},{1,5},{2,6},{3,7},{4,0},{5,1},{6,2},{7,3},{8,12},{9,13},{10,... | collective-permute-start | bytes 786440 | tf_op jit(solution)/shard_map/ppermute | solution.py:14
  172.0 5.0 %collective-permute-start.8 = (bf16[16,4096]{1,0:T(8,128)(2,1)S(1)}, bf16[16,4096]{1,0:T(8,128)(2,1)S(1)}, u32[]{:S(2)}, u32[]{:S(2)}) collective-permute-start(bf16[16,4096]{1,0:T(8,128)(2,1)S(1)} %select_convert_fusion.7), channel_id=1, source_target_pairs={{0,2},{1,3},{2,0},{3,1},{4,6},{5,7},{6,4},{7,5},{8,10},{9,11},{10,... | collective-permute-start | bytes 393224 | tf_op jit(solution)/shard_map/ppermute | solution.py:14
  177.1 1.3 collective-permute-start.9
  178.5 1.3 collective-permute-start.10
  179.8 5.6 %collective-permute-start.11 = (bf16[16,4096]{1,0:T(8,128)(2,1)S(1)}, bf16[16,4096]{1,0:T(8,128)(2,1)S(1)}, u32[]{:S(2)}, u32[]{:S(2)}) collective-permute-start(bf16[16,4096]{1,0:T(8,128)(2,1)S(1)} %maximum_select_fusion.10), channel_id=1, source_target_pairs={{0,2},{1,3},{2,0},{3,1},{4,6},{5,7},{6,4},{7,5},{8,10},{9,11},{10,... | collective-permute-start | bytes 393224 | tf_op jit(solution)/shard_map/ppermute | solution.py:14
  185.5 7.6 %collective-permute-start.12 = (bf16[32,4096]{1,0:T(8,128)(2,1)S(1)}, bf16[32,4096]{1,0:T(8,128)(2,1)S(1)}, u32[]{:S(2)}, u32[]{:S(2)}) collective-permute-start(bf16[32,4096]{1,0:T(8,128)(2,1)S(1)} %maximum_select_fusion.8), channel_id=1, source_target_pairs={{0,4},{1,5},{2,6},{3,7},{4,0},{5,1},{6,2},{7,3},{8,12},{9,13},{10,... | collective-permute-start | bytes 786440 | tf_op jit(solution)/shard_map/ppermute | solution.py:14
  193.2 12.3 %collective-permute-start.13 = (bf16[64,4096]{1,0:T(8,128)(2,1)S(1)}, bf16[64,4096]{1,0:T(8,128)(2,1)S(1)}, u32[]{:S(2)}, u32[]{:S(2)}) collective-permute-start(bf16[64,4096]{1,0:T(8,128)(2,1)S(1)} %maximum_select_fusion.5), channel_id=1, source_target_pairs={{0,8},{1,9},{2,10},{3,11},{4,12},{5,13},{6,14},{7,15},{8,0},{9,1},... | collective-permute-start | bytes 1572872 | tf_op jit(solution)/shard_map/ppermute | solution.py:14
  205.7 46.1 %collective-permute-start.14 = (bf16[128,4096]{1,0:T(8,128)(2,1)S(1)}, bf16[128,4096]{1,0:T(8,128)(2,1)S(1)}, u32[]{:S(2)}, u32[]{:S(2)}) collective-permute-start(bf16[128,4096]{1,0:T(8,128)(2,1)S(1)} %maximum_select_fusion.3), channel_id=1, source_target_pairs={{0,16},{1,17},{2,18},{3,19},{4,20},{5,21},{6,22},{7,23},{8,24},{9,... | collective-permute-start | bytes 3145736 | tf_op jit(solution)/shard_map/ppermute | solution.py:14
  213.1 41.3 %copy-start.17 = (bf16[4096,384]{0,1:T(8,128)(2,1)S(1)}, bf16[4096,384]{0,1:T(8,128)(2,1)}, u32[]{:S(2)}) copy-start(bf16[4096,384]{0,1:T(8,128)(2,1)} %get-tuple-element.19) | copy-start | bytes 9437188
  253.0 1.4 copy-start.6
  253.0 2.9 copy-start.2
  256.0 2.4 copy-start.13
  259.2 2.0 copy-start.4
  261.4 48.4 %collective-permute-start.15 = (bf16[128,4096]{1,0:T(8,128)(2,1)S(1)}, bf16[128,4096]{1,0:T(8,128)(2,1)S(1)}, u32[]{:S(2)}, u32[]{:S(2)}) collective-permute-start(bf16[128,4096]{1,0:T(8,128)(2,1)S(1)} %select_convert_fusion), channel_id=1, source_target_pairs={{0,16},{1,17},{2,18},{3,19},{4,20},{5,21},{6,22},{7,23},{8,24},{9,... | collective-permute-start | bytes 3145736 | tf_op jit(solution)/shard_map/ppermute | solution.py:14
  312.4 2.2 copy-start.1
  312.4 13.9 %collective-permute-start.16 = (bf16[64,4096]{1,0:T(8,128)(2,1)S(1)}, bf16[64,4096]{1,0:T(8,128)(2,1)S(1)}, u32[]{:S(2)}, u32[]{:S(2)}) collective-permute-start(bf16[64,4096]{1,0:T(8,128)(2,1)S(1)} %select_convert_fusion.2), channel_id=1, source_target_pairs={{0,8},{1,9},{2,10},{3,11},{4,12},{5,13},{6,14},{7,15},{8,0},{9,1},... | collective-permute-start | bytes 1572872 | tf_op jit(solution)/shard_map/ppermute | solution.py:14
  326.5 7.4 %collective-permute-start.17 = (bf16[32,4096]{1,0:T(8,128)(2,1)S(1)}, bf16[32,4096]{1,0:T(8,128)(2,1)S(1)}, u32[]{:S(2)}, u32[]{:S(2)}) collective-permute-start(bf16[32,4096]{1,0:T(8,128)(2,1)S(1)} %select_convert_fusion.4), channel_id=1, source_target_pairs={{0,4},{1,5},{2,6},{3,7},{4,0},{5,1},{6,2},{7,3},{8,12},{9,13},{10,... | collective-permute-start | bytes 786440 | tf_op jit(solution)/shard_map/ppermute | solution.py:14
  327.5 7.5 %copy-start.3 = (f32[1,1,256,4096]{2,3,1,0:T(8,128)S(1)}, f32[1,1,256,4096]{2,3,1,0:T(8,128)}, u32[]{:S(2)}) copy-start(f32[1,1,256,4096]{2,3,1,0:T(8,128)} %copy.54) | copy-start | bytes 12582916
  334.1 5.0 %collective-permute-start.18 = (bf16[16,4096]{1,0:T(8,128)(2,1)S(1)}, bf16[16,4096]{1,0:T(8,128)(2,1)S(1)}, u32[]{:S(2)}, u32[]{:S(2)}) collective-permute-start(bf16[16,4096]{1,0:T(8,128)(2,1)S(1)} %select_convert_fusion.6), channel_id=1, source_target_pairs={{0,2},{1,3},{2,0},{3,1},{4,6},{5,7},{6,4},{7,5},{8,10},{9,11},{10,... | collective-permute-start | bytes 393224 | tf_op jit(solution)/shard_map/ppermute | solution.py:14
  339.2 12.8 %collective-permute-start.19 = (bf16[8,4096]{1,0:T(8,128)(2,1)S(1)}, bf16[8,4096]{1,0:T(8,128)(2,1)S(1)}, u32[]{:S(2)}, u32[]{:S(2)}) collective-permute-start(bf16[8,4096]{1,0:T(8,128)(2,1)S(1)} %select_convert_fusion.8), channel_id=1, source_target_pairs={{0,1},{1,0},{2,3},{3,2},{4,5},{5,4},{6,7},{7,6},{8,9},{9,8},{10,11... | collective-permute-start | bytes 196616 | tf_op jit(solution)/shard_map/ppermute | solution.py:14
where the time goes:
time: 354 us; the launch traced here: 353 us
  waiting for transfers between devices  262 us (74%)
  local copies, waits for them, and re-layouts  46.5 us (13%)
  other arithmetic  25.2 us (7%)
  starting transfers between devices  13.3 us (4%)
  matrix products  5.77 us (2%)
    ppermute x20, waiting for transfers between devices, swapped(): lax.ppermute(shard, axis, [(i, i ^ 1 << stride) for i in range(lax.axis_s...  262 us
    unnamed x54, local copies, waits for them, and re-layouts  33.2 us
    ppermute x20, starting transfers between devices, swapped(): lax.ppermute(shard, axis, [(i, i ^ 1 << stride) for i in range(lax.axis_s...  13.3 us
    slice x1, local copies, waits for them, and re-layouts, mixer(): layer_state = state[layer_index, 0].reshape(-1, head_size, head_size)  7.96 us
  transfers between devices with their start and end apart: 20, of which 18 were waited for; matrix products, arithmetic and copies ran while one was open for 12% of the time, Pallas kernels for 0%

commit v1 on v0

--- a/solution.py
+++ b/solution.py
@@ -1,6 +1,10 @@
+import functools
+
 import jax
 import jax.numpy as jnp
 from jax import lax
+from jax.experimental import pallas as pl
+from jax.experimental.pallas import tpu as pltpu
 from jax.sharding import PartitionSpec as P
 
 D = 4096
@@ -182,9 +186,307 @@
     return (mixed[None], new_state)
 
 
+class Place:
+    def __init__(self, n):
+        me = lax.axis_index("tp")
+        self.n, self.planes = n, n // 8
+        self.me = me
+        self.c = me % 2
+        self.x = (me // 2) % 2
+        self.y = (me // 4) % 2
+        self.z = me // 8
+        self.sib = me + 1 - 2 * self.c
+        self.xn = me + 2 * (1 - 2 * self.x)
+        self.yn = me + 4 * (1 - 2 * self.y)
+        self.far = [self.planes // 2] + [k for k in range(1, self.planes) if k != self.planes // 2]
+        self.near = [k for k in self.far if k != self.planes // 2] + [self.planes // 2]
+
+    def plane(self, k):
+        return (self.z + k) % self.planes
+
+    def zn(self, k):
+        return self.plane(k) * 8 + self.me % 8
+
+    def greet(self):
+        barrier = pltpu.get_barrier_semaphore()
+        others = [self.sib, self.xn, self.yn] + [self.zn(k) for k in self.far]
+        for other in others:
+            pl.semaphore_signal(
+                barrier, inc=1, device_id=(other,), device_id_type=pl.DeviceIdType.MESH
+            )
+        pl.semaphore_wait(barrier, len(others))
+
+
+def remote(src, dst, send, recv, to):
+    return pltpu.make_async_remote_copy(
+        src_ref=src,
+        dst_ref=dst,
+        send_sem=send,
+        recv_sem=recv,
+        device_id=(to,),
+        device_id_type=pl.DeviceIdType.MESH,
+    )
+
+
+def gather_sends(n):
+    planes = n // 8
+    return (planes - 1) + 3 * planes + 4 * planes + 2 * planes
+
+
+def gather_phase(at, own_ref, full_ref, send, recv_a, recv_b):
+    half = own_ref.shape[1] // 2
+    first, second = pl.ds(0, half), pl.ds(half, half)
+    started = []
+
+    def tile(p, y, x, c):
+        return ((p * 2 + y) * 2 + x) * 2 + c
+
+    def go(src, t, to, cols=None, recv=recv_a):
+        dst = full_ref.at[t]
+        if cols is not None:
+            src, dst = src.at[:, cols], dst.at[:, cols]
+        copy = remote(src, dst, send.at[len(started)], recv.at[t], to)
+        copy.start()
+        started.append(copy)
+
+    def arrived(t, cols=None, recv=recv_a):
+        dst = full_ref.at[t]
+        if cols is not None:
+            dst = dst.at[:, cols]
+        remote(dst, dst, send.at[0], recv.at[t], at.sib).wait_recv()
+
+    for k in at.near:
+        go(own_ref, at.me, at.zn(k))
+    go(own_ref, at.me, at.xn)
+    go(own_ref, at.me, at.yn)
+    go(own_ref, at.me, at.sib)
+    full_ref[at.me] = own_ref[...]
+
+    def spread(k):
+        p = at.plane(k)
+        t = tile(p, at.y, 1 - at.x, at.c)
+        arrived(t)
+        go(full_ref.at[t], t, at.yn, first, recv_a)
+        go(full_ref.at[t], t, at.sib)
+        t = tile(p, 1 - at.y, at.x, at.c)
+        arrived(t)
+        go(full_ref.at[t], t, at.xn, second, recv_b)
+        go(full_ref.at[t], t, at.sib)
+
+    def corner(k):
+        t = tile(at.plane(k), 1 - at.y, 1 - at.x, at.c)
+        arrived(t, first, recv_a)
+        go(full_ref.at[t], t, at.sib, first, recv_a)
+        arrived(t, second, recv_b)
+        go(full_ref.at[t], t, at.sib, second, recv_b)
+
+    order = [0] + at.near
+    for step, k in enumerate(order):
+        if step:
+            t = at.zn(k)
+            arrived(t)
+            go(full_ref.at[t], t, at.xn)
+            go(full_ref.at[t], t, at.yn)
+            go(full_ref.at[t], t, at.sib)
+        if step >= 1:
+            spread(order[step - 1])
+        if step >= 2:
+            corner(order[step - 2])
+    spread(order[-1])
+    if len(order) > 1:
+        corner(order[-2])
+    corner(order[-1])
+    for k in order:
+        p = at.plane(k)
+        for y in (at.y, 1 - at.y):
+            for x in (at.x, 1 - at.x):
+                t = tile(p, y, x, 1 - at.c)
+                if y is not at.y and x is not at.x:
+                    arrived(t, first, recv_a)
+                    arrived(t, second, recv_b)
+                else:
+                    arrived(t)
+    for copy in started:
+        copy.wait_send()
+
+
+def gather_kernel(n, own_ref, full_ref, send, recv_a, recv_b):
+    at = Place(n)
+    at.greet()
+    gather_phase(at, own_ref, full_ref, send, recv_a, recv_b)
+
+
+def sum_scratch(n, rows, columns):
+    planes, half = n // 8, columns // 2
+    tiles = lambda count, width: pltpu.VMEM((count, rows, width), jnp.bfloat16)
+    return [
+        tiles(n // 2, columns),
+        tiles(n // 2, columns),
+        tiles(planes, half),
+        tiles(planes, half),
+        tiles(planes, columns),
+        tiles(planes, columns),
+        tiles(planes, columns),
+        tiles(planes, columns),
+        pltpu.SemaphoreType.DMA((6 * planes,)),
+        pltpu.SemaphoreType.DMA((6 * planes,)),
+    ]
+
+
+def sum_phase(at, part_ref, scratch):
+    sib, acc, in_a, in_b, in_x, in_y, out_z, in_z, send, recv = scratch
+    planes = at.planes
+    half = part_ref.shape[3] // 2
+    first, second = pl.ds(0, half), pl.ds(half, half)
+    order = at.far + [0]
+    started = []
+
+    def go(src, dst, kind, k, to):
+        copy = remote(src, dst, send.at[kind * planes + k], recv.at[kind * planes + k], to)
+        copy.start()
+        started.append(copy)
+
+    def arrived(dst, kind, k):
+        slot = kind * planes + k
+        remote(dst, dst, send.at[slot], recv.at[slot], at.sib).wait_recv()
+
+    def f32(v):
+        return v.astype(jnp.float32)
+
+    def chunk(p, y, x):
+        return (p * 2 + y) * 2 + x
+
+    for k in order:
+        block = pl.ds(at.plane(k) * 4, 4)
+        go(part_ref.at[block, 1 - at.c], sib.at[block], 0, k, at.sib)
+    for k in order:
+        p = at.plane(k)
+        block = pl.ds(p * 4, 4)
+        arrived(sib.at[block], 0, k)
+        for y, x in ((1 - at.y, 1 - at.x), (at.y, 1 - at.x), (1 - at.y, at.x), (at.y, at.x)):
+            q = chunk(p, y, x)
+            acc[q] = (f32(part_ref[q, at.c]) + f32(sib[q])).astype(jnp.bfloat16)
+            if y is not at.y and x is not at.x:
+                go(acc.at[q, :, first], in_a.at[k], 1, k, at.yn)
+                go(acc.at[q, :, second], in_b.at[k], 2, k, at.xn)
+    for k in order:
+        p = at.plane(k)
+        q = chunk(p, at.y, 1 - at.x)
+        arrived(in_a.at[k], 1, k)
+        acc[q, :, first] = (f32(acc[q, :, first]) + f32(in_a[k])).astype(jnp.bfloat16)
+        go(acc.at[q], in_x.at[k], 3, k, at.xn)
+        q = chunk(p, 1 - at.y, at.x)
+        arrived(in_b.at[k], 2, k)
+        acc[q, :, second] = (f32(acc[q, :, second]) + f32(in_b[k])).astype(jnp.bfloat16)
+        go(acc.at[q], in_y.at[k], 4, k, at.yn)
+    total = None
+    for k in order:
+        arrived(in_x.at[k], 3, k)
+        arrived(in_y.at[k], 4, k)
+        plane = f32(acc[chunk(at.plane(k), at.y, at.x)]) + f32(in_x[k]) + f32(in_y[k])
+        if k:
+            out_z[k] = plane.astype(jnp.bfloat16)
+            go(out_z.at[k], in_z.at[k], 5, k, at.zn(k))
+        else:
+            total = plane
+    for k in at.near:
+        arrived(in_z.at[k], 5, k)
+        total = total + f32(in_z[k])
+    for copy in started:
+        copy.wait_send()
+    return total
+
+
+def middle_kernel(n, part_ref, own_ref, full_ref, next_ref, *scratch):
+    at = Place(n)
+    at.greet()
+    total = sum_phase(at, part_ref, scratch[:10])
+    next_ref[...] = (own_ref[...].astype(jnp.float32) + total).astype(jnp.bfloat16)
+    gather_phase(at, next_ref, full_ref, *scratch[10:])
+
+
+def last_kernel(n, part_ref, own_ref, next_ref, *scratch):
+    at = Place(n)
+    at.greet()
+    total = sum_phase(at, part_ref, scratch)
+    next_ref[...] = (own_ref[...].astype(jnp.float32) + total).astype(jnp.bfloat16)
+
+
+def comm_call(kernel, n, collective_id, out_shape, scratch_shapes, *operands):
+    vmem = pl.BlockSpec(memory_space=pltpu.VMEM)
+    return pl.pallas_call(
+        functools.partial(kernel, n),
+        out_shape=out_shape,
+        in_specs=[vmem] * len(operands),
+        out_specs=jax.tree.map(lambda _: vmem, out_shape),
+        scratch_shapes=scratch_shapes,
+        compiler_params=pltpu.CompilerParams(
+            collective_id=collective_id, has_side_effects=True, vmem_limit_bytes=40 << 20
+        ),
+    )(*operands)
+
+
+def gather_scratch(n):
+    return [
+        pltpu.SemaphoreType.DMA((gather_sends(n),)),
+        pltpu.SemaphoreType.DMA((n,)),
+        pltpu.SemaphoreType.DMA((n,)),
+    ]
+
+
+def on_device_fast(n, *args):
+    tokens, gain, wr, wk, wv, wd, wq, wg, bias, self_w, ro_gain, w_out, state = args
+    own = tokens[0]
+    rows, columns = own.shape
+    head = wr.shape[3]
+    full_shape = jax.ShapeDtypeStruct((n, rows, columns), own.dtype)
+    own_shape = jax.ShapeDtypeStruct(own.shape, own.dtype)
+    position = lax.axis_index("tp")
+    new_state = []
+
+    def mixer(full, layer):
+        x = full.reshape(n * rows, columns)
+        wide = x.astype(jnp.float32)
+        scaled = (wide * gain[layer]).astype(jnp.bfloat16)
+        inv = lax.rsqrt(jnp.mean(wide * wide, axis=1) + RMS_EPS)[:, None]
+        pieces = [
+            jnp.dot(scaled, w[layer, 0], preferred_element_type=jnp.float32) * inv
+            for w in (wr, wk, wv, wd, wq, wg)
+        ]
+        cols = lambda table: lax.dynamic_slice_in_dim(table[layer], position * head, head)
+        o, s = recurrent_update(
+            state[layer, 0].reshape(-1, head, head), *pieces, cols(bias), cols(self_w), cols(ro_gain)
+        )
+        new_state.append(s.reshape(s.shape[0], head * head))
+        part = jnp.dot(o, w_out[layer, 0], preferred_element_type=jnp.float32)
+        return part.astype(jnp.bfloat16).reshape(n // 2, 2, rows, columns)
+
+    full = comm_call(gather_kernel, n, 0, full_shape, gather_scratch(n), own)
+    part = mixer(full, 0)
+    full, own = comm_call(
+        middle_kernel,
+        n,
+        1,
+        (full_shape, own_shape),
+        sum_scratch(n, rows, columns) + gather_scratch(n),
+        part,
+        own,
+    )
+    part = mixer(full, 1)
+    mixed = comm_call(last_kernel, n, 2, own_shape, sum_scratch(n, rows, columns), part, own)
+    return mixed[None], jnp.stack(new_state)[:, None]
+
+
+def pick(n, *args):
+    one_block = args[0].shape[2] == args[1].shape[1]
+    if one_block and n % 16 == 0:
+        return on_device_fast(n, *args)
+    return on_device(*args)
+
+
 def solution(mesh):
     return jax.shard_map(
-        on_device,
+        functools.partial(pick, mesh.shape["tp"]),
         mesh=mesh,
         in_specs=(
             P("tp", None, None),

time: 354 us -> 160 us (0.45)
  waiting for transfers between devices: 262 us -> 0 us
  Pallas kernels: 0 us -> 75.8 us
  matrix products: 5.77 us -> 23.8 us
  starting transfers between devices: 13.3 us -> 0 us
  local copies, waits for them, and re-layouts: 46.5 us -> 37 us
  other arithmetic: 25.2 us -> 21 us
    ppermute x20 -> x0, waiting for transfers between devices: 262 us -> none  [swapped(): lax.ppermute(shard, axis, [(i, i ^ 1 << stride) for i in range(lax.axis_s...]
    pallas_call x0 -> x3, Pallas kernels: none -> 75.8 us  [comm_call(): pl.pallas_call(functools.partial(kernel, n), out_shape=out_shape, in_spec...]
    dot_general x4 -> x12, matrix products: 5.77 us -> 23.8 us  [the longest x10 14 us: mixer(): jnp.dot(scaled, w[layer, 0], preferred_element_type=jnp.float32) * inv]
    ppermute x20 -> x0, starting transfers between devices: 13.3 us -> none  [swapped(): lax.ppermute(shard, axis, [(i, i ^ 1 << stride) for i in range(lax.axis_s...]
    add x8 -> x0, other arithmetic: 6.54 us -> none  [halve_sum(): members = tuple((kept + got for kept, got in zip(keeps, arrived)))]
    unnamed x54 -> x64, local copies, waits for them, and re-layouts: 33.2 us -> 27.3 us
  transfers between devices with their start and end apart: 20 -> 0, of which waited for: 18 -> 0; matrix products, arithmetic and copies ran while one was open for 12% -> 0% of each run, Pallas kernels for 0% -> 0%
where the time goes in v1:
time: 160 us; the launch traced here: 159 us
  Pallas kernels  75.8 us (47%)
  local copies, waits for them, and re-layouts  37 us (23%)
  matrix products  23.8 us (15%)
  other arithmetic  21 us (13%)
    pallas_call x3, Pallas kernels, comm_call(): pl.pallas_call(functools.partial(kernel, n), out_shape=out_shape, in_spec...  75.8 us
    unnamed x64, local copies, waits for them, and re-layouts  27.3 us
    dot_general x10, matrix products, mixer(): jnp.dot(scaled, w[layer, 0], preferred_element_type=jnp.float32) * inv  14 us
    dot_general x2, matrix products, mixer(): part = jnp.dot(o, w_out[layer, 0], preferred_element_type=jnp.float32)  9.8 us
    slice x1, local copies, waits for them, and re-layouts, mixer(): state[layer, 0].reshape(-1, head, head)  7.81 us
    broadcast_in_dim x1, other arithmetic, on_device_fast(): return (mixed[None], jnp.stack(new_state)[:, None])  5.94 us
    add x2, other arithmetic, recurrent_update(): layer_state * shrink[..., None, :]  4.78 us

profile of v1, /device:TPU:0, one launch (start us, length us, event | category | flops | bytes accessed | tf_op | source)
XLA Modules:
  0.0 158.7 jit_solution(12073288560672953811)
XLA Ops:
  0.6 0.8 copy-done.2
  1.5 21.9 %shard_map.140 = bf16[32,8,4096]{2,1,0:T(8,128)(2,1)S(1)} custom-call(bf16[8,4096]{1,0:T(8,128)(2,1)S(1)} %bitcast.142), custom_call_target="tpu_custom_call" | custom-call | tf_op jit(solution)/shard_map/pallas_call | solution.py:417
  23.4 0.9 fusion.127
  24.2 0.5 fusion.1
  24.8 0.1 rsqrt.53
  24.9 0.8 convolution_multiply_fusion.8
  25.6 7.8 %fusion.126 = (f32[1,1,256,4096]{3,2,1,0:T(8,128)}, f32[1,1,256,4096]{3,2,1,0:T(8,128)}) fusion(f32[2,1,256,4096]{3,2,1,0:T(8,128)} %param.25), kind=kLoop, calls=%fused_computation.157 | loop fusion | bytes 16777216 | tf_op jit(solution)/shard_map/slice | solution.py:458
  33.4 5.7 %copy.47 = f32[1,1,256,4096]{2,3,1,0:T(8,128)} copy(f32[1,1,256,4096]{3,2,1,0:T(8,128)} %get-tuple-element.17) | data formatting | bytes 8388608
  39.1 0.8 convolution_multiply_fusion.10
  40.0 1.9 %multiply_reduce_fusion.7 = (f32[256]{0:T(256)S(1)}, f32[256]{0:T(256)S(1)}, f32[256,64]{0,1:T(8,128)S(1)}) fusion(f32[256,64]{0,1:T(8,128)S(1)} %convolution_multiply_fusion.10, f32[64]{0:T(128)S(1)} %get-tuple-element.32, f32[256]{0:T(256)S(1)} %rsqrt.53, bf16[2,1,4096,64]{2,3,1,0:T(8,128)(2,1)} %param.15, bf16[32,8,4096]{2,1,0:T(8,128)(2,1)S(1)} %shard_map.140, ...), kind=kOutput, calls=%fused_computation.112 | convolution fusion | flops 137461248 | bytes 2772224 | tf_op jit(solution)/shard_map/dot_general | solution.py:453
  42.0 2.0 %fusion.80 = f32[256,64]{0,1:T(8,128)S(1)} fusion(bf16[2,1,4096,64]{2,3,1,0:T(8,128)(2,1)} %param.18, bf16[32,8,4096]{2,1,0:T(8,128)(2,1)S(1)} %shard_map.140, f32[4096]{0:T(1024)S(1)} %bitcast.158, f32[256]{0:T(256)S(1)} %rsqrt.53, f32[64]{0:T(128)S(1)} %get-tuple-element.35), kind=kOutput, calls=%fused_computation.97 | convolution fusion | flops 137560064 | bytes 2704640 | tf_op jit(solution)/shard_map/dot_general | solution.py:453
  44.1 0.8 fusion.125
  44.9 0.7 multiply_reduce_fusion.3
  45.6 1.5 multiply_reduce_fusion.2
  47.1 0.6 fusion.118
  47.9 4.9 %convolution_convert_fusion.1 = bf16[256,4096]{1,0:T(8,128)(2,1)} fusion(bf16[32,8,4096]{2,1,0:T(8,128)(2,1)S(1)} %shard_map.140, f32[4096]{0:T(1024)S(1)} %bitcast.160, bf16[2,1,64,4096]{3,2,1,0:T(8,128)(2,1)S(1)} %copy-done.8, bf16[2,1,4096,64]{2,3,1,0:T(8,128)(2,1)} %param.20, f32[256,64]{0,1:T(8,128)S(1)} %convolution_multiply_fusion.8, ...), kind=kOutput, calls=%fused_computation.6 | convolution fusion | flops 272809984 | bytes 5394944 | tf_op jit(solution)/shard_map/dot_general | solution.py:461
  52.8 1.6 %copy-done = bf16[256,4096]{1,0:T(8,128)(2,1)S(1)} copy-done((bf16[256,4096]{1,0:T(8,128)(2,1)S(1)}, bf16[256,4096]{1,0:T(8,128)(2,1)}, u32[]{:S(2)}) %copy-start) | copy-done | bytes 2097176
  54.4 35.5 %shard_map.141 = (bf16[32,8,4096]{2,1,0:T(8,128)(2,1)S(1)}, bf16[8,4096]{1,0:T(8,128)(2,1)S(1)}) custom-call(bf16[16,2,8,4096]{3,2,1,0:T(8,128)(2,1)S(1)} %bitcast.140, bf16[8,4096]{1,0:T(8,128)(2,1)S(1)} %bitcast.143), custom_call_target="tpu_custom_call" | custom-call | tf_op jit(solution)/shard_map/pallas_call | solution.py:417
  89.9 0.5 fusion.3
  90.4 0.1 rsqrt.57
  90.5 1.8 %convolution_multiply_fusion.2 = f32[256,64]{0,1:T(8,128)S(1)} fusion(bf16[32,8,4096]{2,1,0:T(8,128)(2,1)S(1)} %get-tuple-element.4, f32[4096]{0:T(1024)S(1)} %bitcast.149, bf16[2,1,4096,64]{2,3,1,0:T(8,128)(2,1)} %param.17, f32[256]{0:T(256)S(1)} %rsqrt.57), kind=kOutput, calls=%fused_computation.34 | convolution fusion | flops 137379840 | bytes 2704384 | tf_op jit(solution)/shard_map/dot_general | solution.py:453
  92.3 5.6 %copy.46 = f32[1,1,256,4096]{2,3,1,0:T(8,128)} copy(f32[1,1,256,4096]{3,2,1,0:T(8,128)} %get-tuple-element.16) | data formatting | bytes 8388608
  97.9 1.9 %convolution_multiply_fusion.4 = f32[256,64]{0,1:T(8,128)S(1)} fusion(bf16[32,8,4096]{2,1,0:T(8,128)(2,1)S(1)} %get-tuple-element.4, f32[4096]{0:T(1024)S(1)} %bitcast.150, bf16[2,1,4096,64]{2,3,1,0:T(8,128)(2,1)} %param.16, f32[256]{0:T(256)S(1)} %rsqrt.57), kind=kOutput, calls=%fused_computation.40 | convolution fusion | flops 137379840 | bytes 2704384 | tf_op jit(solution)/shard_map/dot_general | solution.py:453
  99.8 2.5 %multiply_reduce_fusion.4 = (f32[256]{0:T(256)}, f32[256]{0:T(256)S(1)}, f32[256,64]{0,1:T(8,128)S(1)}) fusion(f32[256,64]{0,1:T(8,128)S(1)} %convolution_multiply_fusion.4, f32[64]{0:T(128)S(1)} %get-tuple-element.33, f32[256]{0:T(256)S(1)} %rsqrt.57, bf16[2,1,4096,64]{2,3,1,0:T(8,128)(2,1)} %param.15, bf16[32,8,4096]{2,1,0:T(8,128)(2,1)S(1)} %get-tuple-element.4, ...), kind=kOutput, calls=%fused_computation.105 | convolution fusion | flops 137461248 | bytes 2772224 | tf_op jit(solution)/shard_map/dot_general | solution.py:453
  102.3 0.8 fusion.85
  103.2 0.8 fusion.124
  104.0 0.5 copy-done.6
  104.5 0.7 multiply_reduce_fusion.1
  105.2 1.5 multiply_reduce_fusion
  106.7 0.6 reduce_sum.97
  107.3 0.7 broadcast_multiply_fusion.6
  107.9 0.5 copy-done.23
  108.5 0.5 add_rsqrt_fusion.2
  109.0 4.9 %convolution_convert_fusion = bf16[256,4096]{1,0:T(8,128)(2,1)} fusion(bf16[32,8,4096]{2,1,0:T(8,128)(2,1)S(1)} %get-tuple-element.4, f32[4096]{0:T(1024)S(1)} %bitcast.154, bf16[2,1,64,4096]{3,2,1,0:T(8,128)(2,1)S(1)} %copy-done.8, bf16[2,1,4096,64]{2,3,1,0:T(8,128)(2,1)} %param.20, f32[256,64]{0,1:T(8,128)S(1)} %convolution_multiply_fusion.2, ...), kind=kOutput, calls=%fused_computation.5 | convolution fusion | flops 272809984 | bytes 5394944 | tf_op jit(solution)/shard_map/dot_general | solution.py:461
  113.9 1.6 %copy-done.1 = bf16[256,4096]{1,0:T(8,128)(2,1)S(1)} copy-done((bf16[256,4096]{1,0:T(8,128)(2,1)S(1)}, bf16[256,4096]{1,0:T(8,128)(2,1)}, u32[]{:S(2)}) %copy-start.1) | copy-done | bytes 2097176
  115.5 18.4 %shard_map.142 = bf16[8,4096]{1,0:T(8,128)(2,1)S(1)} custom-call(bf16[16,2,8,4096]{3,2,1,0:T(8,128)(2,1)S(1)} %bitcast.141, bf16[8,4096]{1,0:T(8,128)(2,1)S(1)} %get-tuple-element.5.own_ref), custom_call_target="tpu_custom_call" | custom-call | tf_op jit(solution)/shard_map/pallas_call | solution.py:417
  134.0 1.5 broadcast_multiply_fusion
  135.5 0.5 broadcast_multiply_fusion.1
  136.0 0.2 copy-done.7
  136.2 1.4 bitcast_add_fusion
  137.6 0.5 broadcast_multiply_fusion.2
  138.2 0.3 copy-done.12
  138.4 0.5 broadcast_multiply_fusion.3
  139.0 0.9 copy-done.5
  139.8 3.4 %bitcast_add_fusion.1 = f32[1,256,4096]{1,2,0:T(8,128)} fusion(f32[256,64,64]{0,2,1:T(8,128)S(1)} %broadcast_multiply_fusion.2, f32[256,64,64]{0,2,1:T(8,128)S(1)} %broadcast_multiply_fusion.3, f32[1,1,256,4096]{2,3,1,0:T(8,128)S(1)} %copy-done.5, f32[256,64]{0,1:T(8,128)S(1)} %copy-done.10), kind=kLoop, calls=%fused_computation.14 | loop fusion | flops 3145728 | bytes 16842752 | tf_op jit(solution)/shard_map/add | solution.py:47
  143.2 5.9 %maximum_bitcast_fusion = f32[2,1,256,4096]{2,3,0,1:T(8,128)} fusion(f32[1,256,4096]{1,2,0:T(8,128)S(1)} %bitcast_add_fusion, f32[1,256,4096]{1,2,0:T(8,128)} %bitcast_add_fusion.1), kind=kLoop, calls=%fused_computation | loop fusion | flops 2097152 | bytes 16777216 | tf_op jit(solution)/shard_map/broadcast_in_dim | solution.py:477
  149.2 8.9 %copy.25 = f32[2,1,256,4096]{3,2,1,0:T(8,128)} copy(f32[2,1,256,4096]{2,3,0,1:T(8,128)} %maximum_bitcast_fusion) | data formatting | bytes 16777216
  158.1 0.6 copy.57
  (66 shorter events, 0.4 us)
Async XLA Ops:
  0.6 0.8 copy-start.2
  1.5 23.4 %copy-start.25 = (bf16[2,1,4096,64]{2,3,1,0:T(8,128)(2,1)S(1)}, bf16[2,1,4096,64]{2,3,1,0:T(8,128)(2,1)}, u32[]{:S(2)}) copy-start(bf16[2,1,4096,64]{2,3,1,0:T(8,128)(2,1)} %param.17) | copy-start | bytes 3145732
  33.4 5.7 %copy-start.26 = (bf16[2,1,4096,64]{2,3,1,0:T(8,128)(2,1)S(1)}, bf16[2,1,4096,64]{2,3,1,0:T(8,128)(2,1)}, u32[]{:S(2)}) copy-start(bf16[2,1,4096,64]{2,3,1,0:T(8,128)(2,1)} %param.16) | copy-start | bytes 3145732
  33.4 6.5 %copy-start.20 = (f32[2,2048]{1,0:T(2,128)S(1)}, f32[2,2048]{1,0:T(2,128)}, u32[]{:S(2)}) copy-start(f32[2,2048]{1,0:T(2,128)} %param.22) | copy-start | bytes 49156
  39.1 2.8 %copy-start.21 = (f32[2,2048]{1,0:T(2,128)S(1)}, f32[2,2048]{1,0:T(2,128)}, u32[]{:S(2)}) copy-start(f32[2,2048]{1,0:T(2,128)} %param.21) | copy-start | bytes 49156
  39.9 4.2 %copy-start.28 = (bf16[2,1,4096,64]{2,3,1,0:T(8,128)(2,1)S(1)}, bf16[2,1,4096,64]{2,3,1,0:T(8,128)(2,1)}, u32[]{:S(2)}) copy-start(bf16[2,1,4096,64]{2,3,1,0:T(8,128)(2,1)} %param.19) | copy-start | bytes 3145732
  41.9 3.0 %copy-start.4 = (f32[1,1,256,4096]{2,3,1,0:T(8,128)S(1)}, f32[1,1,256,4096]{2,3,1,0:T(8,128)}, u32[]{:S(2)}) copy-start(f32[1,1,256,4096]{2,3,1,0:T(8,128)} %copy.47) | copy-start | bytes 12582916
  44.0 3.0 %copy-start.9 = (f32[256,64]{0,1:T(8,128)}, f32[256,64]{0,1:T(8,128)S(1)}, u32[]{:S(2)}) copy-start(f32[256,64]{0,1:T(8,128)S(1)} %fusion.80) | copy-start | bytes 196612
  44.9 2.2 %copy-start.11 = (f32[256,64]{0,1:T(8,128)}, f32[256,64]{0,1:T(8,128)S(1)}, u32[]{:S(2)}) copy-start(f32[256,64]{0,1:T(8,128)S(1)} %get-tuple-element.14) | copy-start | bytes 196612
  44.9 2.2 %copy-start.13 = (f32[256,64]{0,1:T(8,128)}, f32[256,64]{0,1:T(8,128)S(1)}, u32[]{:S(2)}) copy-start(f32[256,64]{0,1:T(8,128)S(1)} %get-tuple-element.19) | copy-start | bytes 196612
  44.9 2.2 %copy-start.22 = (f32[2,2048]{1,0:T(2,128)S(1)}, f32[2,2048]{1,0:T(2,128)}, u32[]{:S(2)}) copy-start(f32[2,2048]{1,0:T(2,128)} %param.23) | copy-start | bytes 49156
  44.9 3.0 %copy-start.8 = (bf16[2,1,64,4096]{3,2,1,0:T(8,128)(2,1)S(1)}, bf16[2,1,64,4096]{3,2,1,0:T(8,128)(2,1)}, u32[]{:S(2)}) copy-start(bf16[2,1,64,4096]{3,2,1,0:T(8,128)(2,1)} %param.24) | copy-start | bytes 3145732
  45.6 7.2 %copy-start.3 = (bf16[1,8,4096]{2,1,0:T(8,128)(2,1)S(1)}, bf16[1,8,4096]{2,1,0:T(8,128)(2,1)}, u32[]{:S(2)}) copy-start(bf16[1,8,4096]{2,1,0:T(8,128)(2,1)} %param.13) | copy-start | bytes 196612
  52.8 1.6 %copy-start = (bf16[256,4096]{1,0:T(8,128)(2,1)S(1)}, bf16[256,4096]{1,0:T(8,128)(2,1)}, u32[]{:S(2)}) copy-start(bf16[256,4096]{1,0:T(8,128)(2,1)} %convolution_convert_fusion.1) | copy-start | bytes 6291460
  90.5 12.7 %copy-start.24 = (f32[256]{0:T(256)}, f32[256]{0:T(256)S(1)}, u32[]{:S(2)}) copy-start(f32[256]{0:T(256)S(1)} %rsqrt.57) | copy-start | bytes 3076
  97.9 4.4 %copy-start.27 = (bf16[2,1,4096,64]{2,3,1,0:T(8,128)(2,1)S(1)}, bf16[2,1,4096,64]{2,3,1,0:T(8,128)(2,1)}, u32[]{:S(2)}) copy-start(bf16[2,1,4096,64]{2,3,1,0:T(8,128)(2,1)} %param.18) | copy-start | bytes 3145732
  99.8 3.4 %copy-start.29 = (bf16[2,1,4096,64]{2,3,1,0:T(8,128)(2,1)S(1)}, bf16[2,1,4096,64]{2,3,1,0:T(8,128)(2,1)}, u32[]{:S(2)}) copy-start(bf16[2,1,4096,64]{2,3,1,0:T(8,128)(2,1)} %param.19) | copy-start | bytes 3145732
  102.3 2.2 %copy-start.6 = (f32[1,1,256,4096]{2,3,1,0:T(8,128)S(1)}, f32[1,1,256,4096]{2,3,1,0:T(8,128)}, u32[]{:S(2)}) copy-start(f32[1,1,256,4096]{2,3,1,0:T(8,128)} %copy.46) | copy-start | bytes 12582916
  103.1 3.5 %copy-start.15 = (f32[256,64]{0,1:T(8,128)}, f32[256,64]{0,1:T(8,128)S(1)}, u32[]{:S(2)}) copy-start(f32[256,64]{0,1:T(8,128)S(1)} %fusion.85) | copy-start | bytes 196612
  104.0 2.7 %copy-start.17 = (f32[256,64]{0,1:T(8,128)}, f32[256,64]{0,1:T(8,128)S(1)}, u32[]{:S(2)}) copy-start(f32[256,64]{0,1:T(8,128)S(1)} %get-tuple-element.12) | copy-start | bytes 196612
  104.0 2.7 %copy-start.19 = (f32[256,64]{0,1:T(8,128)}, f32[256,64]{0,1:T(8,128)S(1)}, u32[]{:S(2)}) copy-start(f32[256,64]{0,1:T(8,128)S(1)} %get-tuple-element.18) | copy-start | bytes 196612
  107.9 0.5 copy-start.23
  113.9 1.6 %copy-start.1 = (bf16[256,4096]{1,0:T(8,128)(2,1)S(1)}, bf16[256,4096]{1,0:T(8,128)(2,1)}, u32[]{:S(2)}) copy-start(bf16[256,4096]{1,0:T(8,128)(2,1)} %convolution_convert_fusion) | copy-start | bytes 6291460
  115.5 20.0 %copy-start.18 = (f32[256,64]{0,1:T(8,128)S(1)}, f32[256,64]{0,1:T(8,128)}, u32[]{:S(2)}) copy-start(f32[256,64]{0,1:T(8,128)} %copy-done.17) | copy-start | bytes 196612
  134.0 2.2 %copy-start.7 = (f32[1,1,256,4096]{2,3,1,0:T(8,128)S(1)}, f32[1,1,256,4096]{2,3,1,0:T(8,128)}, u32[]{:S(2)}) copy-start(f32[1,1,256,4096]{2,3,1,0:T(8,128)} %copy.46) | copy-start | bytes 12582916
  134.0 2.2 %copy-start.16 = (f32[256,64]{0,1:T(8,128)S(1)}, f32[256,64]{0,1:T(8,128)}, u32[]{:S(2)}) copy-start(f32[256,64]{0,1:T(8,128)} %copy-done.15) | copy-start | bytes 196612
  136.2 1.4 copy-start.14
  137.6 0.8 copy-start.12
  137.6 2.2 %copy-start.5 = (f32[1,1,256,4096]{2,3,1,0:T(8,128)S(1)}, f32[1,1,256,4096]{2,3,1,0:T(8,128)}, u32[]{:S(2)}) copy-start(f32[1,1,256,4096]{2,3,1,0:T(8,128)} %copy.47) | copy-start | bytes 12582916
  137.6 2.2 %copy-start.10 = (f32[256,64]{0,1:T(8,128)S(1)}, f32[256,64]{0,1:T(8,128)}, u32[]{:S(2)}) copy-start(f32[256,64]{0,1:T(8,128)} %copy-done.9) | copy-start | bytes 196612

commit v2 on v1

--- a/solution.py
+++ b/solution.py
@@ -434,35 +434,174 @@
     ]
 
 
+def lanes(v, times):
+    return jnp.concatenate([v] * times, axis=1)
+
+
+def project_kernel(x_ref, gain_ref, *refs):
+    weights, (out_ref, acc, squares) = refs[:6], refs[6:]
+    step, last = pl.program_id(0), pl.num_programs(0) - 1
+    width = x_ref.shape[2]
+    wide = x_ref[...].astype(jnp.float32).reshape(-1, width)
+    scaled = (wide * gain_ref[...]).astype(jnp.bfloat16)
+    joined = jnp.concatenate([w[0, 0] for w in weights], axis=0)
+    part = lax.dot_general(
+        scaled, joined, (((1,), (1,)), ((), ())), preferred_element_type=jnp.float32
+    )
+    square = wide * wide
+    folded = square[:, :128]
+    for at in range(128, width, 128):
+        folded = folded + square[:, at : at + 128]
+
+    @pl.when(step == 0)
+    def _():
+        acc[...] = part
+        squares[...] = folded
+
+    @pl.when(step > 0)
+    def _():
+        acc[...] += part
+        squares[...] += folded
+
+    @pl.when(step == last)
+    def _():
+        mean = jnp.sum(squares[...], axis=1, keepdims=True) / (width * (last + 1))
+        out_ref[...] = acc[...] * lax.rsqrt(mean + RMS_EPS)
+
+
+def project(full, gain, weights, layer):
+    n, rows, columns = full.shape
+    head = weights[0].shape[2]
+    chunk = columns // 8
+    return pl.pallas_call(
+        project_kernel,
+        grid=(columns // chunk,),
+        in_specs=[
+            pl.BlockSpec((n, rows, chunk), lambda i: (0, 0, i)),
+            pl.BlockSpec((1, chunk), lambda i: (0, i)),
+        ]
+        + [pl.BlockSpec((1, 1, head, chunk), lambda i: (layer, 0, 0, i))] * 6,
+        out_specs=pl.BlockSpec((n * rows, 6 * head), lambda i: (0, 0)),
+        out_shape=jax.ShapeDtypeStruct((n * rows, 6 * head), jnp.float32),
+        scratch_shapes=[
+            pltpu.VMEM((n * rows, 6 * head), jnp.float32),
+            pltpu.VMEM((n * rows, 128), jnp.float32),
+        ],
+        compiler_params=pltpu.CompilerParams(vmem_limit_bytes=32 << 20),
+    )(full, gain[layer][None], *weights)
+
+
+def state_kernel(proj_ref, state_ref, table_ref, w_ref, spread_ref, *refs):
+    part_ref, new_ref = refs[-2:]
+    head = table_ref.shape[1]
+    rows, flat = state_ref.shape[2:]
+    chunk = 8 * head
+    r, k, v, p, q, g = [proj_ref[:, i * head : (i + 1) * head] for i in range(6)]
+    decay = jnp.exp(-jax.nn.sigmoid(table_ref[0:1] + p) * jnp.exp(jnp.float32(-0.5)))
+    rate = jax.nn.sigmoid(q)
+    kn = k * lax.rsqrt(jnp.sum(k * k, axis=1, keepdims=True) + 1.0)
+    taken, added = kn * rate, k * rate
+    kn_w, u_w = lanes(kn, chunk // head), lanes(decay * r, chunk // head)
+    sums = jnp.zeros((2 * rows, head), jnp.float32)
+    for at in range(0, flat, chunk):
+        s = state_ref[0, 0, :, at : at + chunk]
+        both = jnp.concatenate([s * kn_w, s * u_w], axis=0).astype(jnp.bfloat16)
+        sums += lax.dot_general(
+            both,
+            spread_ref[:head, at : at + chunk],
+            (((1,), (1,)), ((), ())),
+            preferred_element_type=jnp.float32,
+        )
+    removed, read = sums[:rows], sums[rows:]
+    read = (
+        read
+        - removed * jnp.sum(taken * r, axis=1, keepdims=True)
+        + v * jnp.sum(added * r, axis=1, keepdims=True)
+    )
+    center = jnp.mean(read, axis=1, keepdims=True)
+    off = read - center
+    spread = jnp.mean(off * off, axis=1, keepdims=True)
+    normed = off * lax.rsqrt(spread + GROUP_EPS) * table_ref[2:3]
+    own_term = jnp.sum(r * k * table_ref[1:2], axis=1, keepdims=True) * v
+    o = ((normed + own_term) * jax.nn.sigmoid(g)).astype(jnp.bfloat16)
+
+    pair = jnp.concatenate([removed, v], axis=0)
+    high = pair.astype(jnp.bfloat16)
+    low = (pair - high.astype(jnp.float32)).astype(jnp.bfloat16)
+    pair = jnp.concatenate([high, low], axis=1)
+    decay_w, taken_w, added_w = [lanes(t, chunk // head) for t in (decay, taken, added)]
+    columns = w_ref.shape[3]
+    for at in range(0, columns, chunk):
+        part = jnp.dot(o, w_ref[0, 0, :, at : at + chunk], preferred_element_type=jnp.float32)
+        part = part.reshape(part_ref.shape[:3] + (chunk,))
+        part_ref[:, :, :, at : at + chunk] = part.astype(jnp.bfloat16)
+    for at in range(0, flat, chunk):
+        wide = jnp.dot(pair, spread_ref[:, at : at + chunk], preferred_element_type=jnp.float32)
+        new_ref[0, 0, :, at : at + chunk] = (
+            state_ref[0, 0, :, at : at + chunk] * decay_w
+            - wide[:rows] * taken_w
+            + wide[rows:] * added_w
+        )
+
+
+def state_step(n, tile_rows, proj, state, table, w_out, spread, layer, earlier):
+    seqs, flat = state.shape[2:]
+    head, columns = w_out.shape[2:]
+    rows = seqs // 2
+    state_spec = pl.BlockSpec((1, 1, rows, flat), lambda i: (layer, 0, i, 0))
+    whole = lambda a: pl.BlockSpec(a.shape, lambda i: (0,) * a.ndim)
+    operands = [proj, state, table, w_out, spread]
+    in_specs = [
+        pl.BlockSpec((rows, proj.shape[1]), lambda i: (i, 0)),
+        state_spec,
+        whole(table),
+        pl.BlockSpec((1, 1, head, columns), lambda i: (layer, 0, 0, 0)),
+        whole(spread),
+    ]
+    if earlier is not None:
+        operands.append(earlier)
+        in_specs.append(pl.BlockSpec(memory_space=pl.ANY))
+    per = rows // tile_rows // 2
+    return pl.pallas_call(
+        state_kernel,
+        grid=(2,),
+        in_specs=in_specs,
+        out_specs=(
+            pl.BlockSpec((per, 2, tile_rows, columns), lambda i: (i, 0, 0, 0)),
+            state_spec,
+        ),
+        out_shape=(
+            jax.ShapeDtypeStruct((n // 2, 2, tile_rows, columns), jnp.bfloat16),
+            jax.ShapeDtypeStruct(state.shape, jnp.float32),
+        ),
+        input_output_aliases={} if earlier is None else {5: 1},
+        compiler_params=pltpu.CompilerParams(vmem_limit_bytes=48 << 20),
+    )(*operands)
+
+
 def on_device_fast(n, *args):
     tokens, gain, wr, wk, wv, wd, wq, wg, bias, self_w, ro_gain, w_out, state = args
+    weights = [jnp.swapaxes(w, 2, 3) for w in (wr, wk, wv, wd, wq, wg)]
     own = tokens[0]
     rows, columns = own.shape
     head = wr.shape[3]
+    flat = state.shape[3]
     full_shape = jax.ShapeDtypeStruct((n, rows, columns), own.dtype)
     own_shape = jax.ShapeDtypeStruct(own.shape, own.dtype)
     position = lax.axis_index("tp")
-    new_state = []
-
-    def mixer(full, layer):
-        x = full.reshape(n * rows, columns)
-        wide = x.astype(jnp.float32)
-        scaled = (wide * gain[layer]).astype(jnp.bfloat16)
-        inv = lax.rsqrt(jnp.mean(wide * wide, axis=1) + RMS_EPS)[:, None]
-        pieces = [
-            jnp.dot(scaled, w[layer, 0], preferred_element_type=jnp.float32) * inv
-            for w in (wr, wk, wv, wd, wq, wg)
-        ]
-        cols = lambda table: lax.dynamic_slice_in_dim(table[layer], position * head, head)
-        o, s = recurrent_update(
-            state[layer, 0].reshape(-1, head, head), *pieces, cols(bias), cols(self_w), cols(ro_gain)
-        )
-        new_state.append(s.reshape(s.shape[0], head * head))
-        part = jnp.dot(o, w_out[layer, 0], preferred_element_type=jnp.float32)
-        return part.astype(jnp.bfloat16).reshape(n // 2, 2, rows, columns)
+    tables = jnp.stack([bias, self_w, ro_gain], axis=1)
+    tables = lax.dynamic_slice_in_dim(tables, position * head, head, 2)
+    value_of = jnp.arange(flat) // head
+    spread = (jnp.arange(2 * head)[:, None] % head == value_of[None]).astype(jnp.bfloat16)
+
+    def mixer(full, layer, earlier):
+        proj = project(full, gain, weights, layer)
+        return state_step(
+            n, rows, proj, state, tables[layer], w_out, spread, layer, earlier
+        )
 
     full = comm_call(gather_kernel, n, 0, full_shape, gather_scratch(n), own)
-    part = mixer(full, 0)
+    part, new_state = mixer(full, 0, None)
     full, own = comm_call(
         middle_kernel,
         n,
@@ -472,9 +611,9 @@
         part,
         own,
     )
-    part = mixer(full, 1)
+    part, new_state = mixer(full, 1, new_state)
     mixed = comm_call(last_kernel, n, 2, own_shape, sum_scratch(n, rows, columns), part, own)
-    return mixed[None], jnp.stack(new_state)[:, None]
+    return mixed[None], new_state
 
 
 def pick(n, *args):

time: 160 us -> 112 us (0.70)
  local copies, waits for them, and re-layouts: 37 us -> 8.42 us
  Pallas kernels: 75.8 us -> 102 us
  matrix products: 23.8 us -> 0 us
  other arithmetic: 21 us -> 0.35 us
    pallas_call x0 -> x4, Pallas kernels: none -> 25.7 us  [the longest x2 18.4 us: state_step(): pl.pallas_call(state_kernel, grid=(2,), in_specs=in_specs, out_specs=(pl....]
    dot_general x12 -> x0, matrix products: 23.8 us -> none  [the longest x10 14 us: mixer(): jnp.dot(scaled, w[layer, 0], preferred_element_type=jnp.float32) * inv]
    unnamed x64 -> x25, local copies, waits for them, and re-layouts: 27.3 us -> 5.17 us
    slice x5 -> x1, local copies, waits for them, and re-layouts: 8.72 us -> 0.87 us  [project(): gain[layer][None]]
    broadcast_in_dim x1 -> x0, other arithmetic: 5.94 us -> none  [on_device_fast(): return (mixed[None], jnp.stack(new_state)[:, None])]
    add x2 -> x0, other arithmetic: 4.78 us -> none  [recurrent_update(): layer_state * shrink[..., None, :]]
    dot_general x4 -> x0, other arithmetic: 4.26 us -> none  [the longest x2 2.95 us: recurrent_update(): jnp.einsum('...ij,...j->...i', layer_state, receptance_vector, precision=...]
    mul x4 -> x0, other arithmetic: 3.05 us -> none  [the longest x2 2.02 us: recurrent_update(): value_vector[..., :, None] * (key_vector * rate)[..., None, :]]
where the time goes in v2:
time: 112 us; the launch traced here: 111 us
  Pallas kernels  102 us (91%)
  local copies, waits for them, and re-layouts  8.42 us (8%)
    pallas_call x3, Pallas kernels, comm_call(): pl.pallas_call(functools.partial(kernel, n), out_shape=out_shape, in_spec...  75.9 us
    pallas_call x2, Pallas kernels, state_step(): pl.pallas_call(state_kernel, grid=(2,), in_specs=in_specs, out_specs=(pl....  18.4 us
    pallas_call x2, Pallas kernels, project(): pl.pallas_call(project_kernel, grid=(columns // chunk,), in_specs=[pl.Blo...  7.35 us
    unnamed x25, local copies, waits for them, and re-layouts  5.17 us
    another operation x3, local copies, waits for them, and re-layouts, on_device_fast(): tables = jnp.stack([bias, self_w, ro_gain], axis=1)  2.37 us

profile of v2, /device:TPU:0, one launch (start us, length us, event | category | flops | bytes accessed | tf_op | source)
XLA Modules:
  0.0 111.2 jit_solution(11355059066843297098)
XLA Ops:
  0.6 0.0 copy-start.2
  0.6 0.0 copy-start.1
  0.7 0.0 copy-start
  0.7 0.9 stack.12
  1.6 0.8 stack.13
  2.3 0.7 stack.14
  3.1 0.1 fusion.4
  3.2 0.9 fusion.5
  4.0 0.3 compare_convert_fusion.spread_ref
  4.3 0.0 copy-start.10
  4.3 0.8 copy-done.10
  5.1 21.9 %shard_map.140.x_ref = bf16[32,8,4096]{2,1,0:T(8,128)(2,1)S(1)} custom-call(bf16[8,4096]{1,0:T(8,128)(2,1)S(1)} %bitcast.24), custom_call_target="tpu_custom_call" | custom-call | tf_op jit(solution)/shard_map/pallas_call | solution.py:417
  27.0 0.0 copy-done.2
  27.0 0.0 copy-done.1
  27.1 0.0 copy-done
  27.1 0.0 copy-start.3
  27.1 1.2 %copy-done.3 = bf16[2,1,4096,64]{2,3,1,0:T(8,128)(2,1)S(1)} copy-done((bf16[2,1,4096,64]{2,3,1,0:T(8,128)(2,1)S(1)}, bf16[2,1,4096,64]{2,3,1,0:T(8,128)(2,1)}, u32[]{:S(2)}) %copy-start.3) | copy-done | bytes 1048600
  28.3 0.0 copy-start.5
  28.3 1.2 %copy-done.5 = bf16[2,1,4096,64]{2,3,1,0:T(8,128)(2,1)S(1)} copy-done((bf16[2,1,4096,64]{2,3,1,0:T(8,128)(2,1)S(1)}, bf16[2,1,4096,64]{2,3,1,0:T(8,128)(2,1)}, u32[]{:S(2)}) %copy-start.5) | copy-done | bytes 1048600
  29.5 0.0 copy-start.7
  29.5 1.2 %copy-done.7 = bf16[2,1,4096,64]{2,3,1,0:T(8,128)(2,1)S(1)} copy-done((bf16[2,1,4096,64]{2,3,1,0:T(8,128)(2,1)S(1)}, bf16[2,1,4096,64]{2,3,1,0:T(8,128)(2,1)}, u32[]{:S(2)}) %copy-start.7) | copy-done | bytes 1048600
  30.7 0.0 copy-start.9
  30.7 3.7 %shard_map.141.proj_ref = f32[256,384]{1,0:T(8,128)S(1)} custom-call(bf16[32,8,4096]{2,1,0:T(8,128)(2,1)S(1)} %shard_map.140.x_ref, f32[1,4096]{1,0:T(1,128)S(1)} %get-tuple-element.15.gain_ref, bf16[2,1,64,4096]{3,2,1,0:T(8,128)(2,1)S(1)} %bitcast.12, bf16[2,1,64,4096]{3,2,1,0:T(8,128)(2,1)S(1)} %bitcast.14, bf16[2,1,64,4096]{3,2,1,0:T(8,128)(2,1)S(1)} %bitcast.16, ...), custom_call_target="tpu_custom_call" | custom-call | tf_op jit(solution)/shard_map/pallas_call | solution.py:476
  34.4 0.0 copy-done.9
  34.4 0.0 copy-start.11
  34.4 0.0 copy-start.8
  34.5 9.2 %shard_map.142 = (bf16[16,2,8,4096]{3,2,1,0:T(8,128)(2,1)S(1)}, f32[2,1,256,4096]{3,2,1,0:T(8,128)}) custom-call(f32[256,384]{1,0:T(8,128)S(1)} %shard_map.141.proj_ref, f32[2,1,256,4096]{3,2,1,0:T(8,128)} %state_ref.3, f32[3,64]{1,0:T(4,128)S(1)} %get-tuple-element.17.table_ref, bf16[2,1,64,4096]{3,2,1,0:T(8,128)(2,1)S(1)} %copy-done.9, ...), custom_call_target="tpu_custom_call" | custom-call | tf_op jit(solution)/shard_map/pallas_call | solution.py:565
  43.7 0.0 copy-start.4
  43.7 0.0 copy-start.6
  43.7 0.0 copy-done.11
  43.7 35.6 %shard_map.143 = (bf16[32,8,4096]{2,1,0:T(8,128)(2,1)S(1)}, bf16[8,4096]{1,0:T(8,128)(2,1)S(1)}) custom-call(bf16[16,2,8,4096]{3,2,1,0:T(8,128)(2,1)S(1)} %get-tuple-element.8.part_ref, bf16[8,4096]{1,0:T(8,128)(2,1)S(1)} %bitcast.25), custom_call_target="tpu_custom_call" | custom-call | tf_op jit(solution)/shard_map/pallas_call | solution.py:417
  79.3 0.0 copy-done.8
  79.3 0.0 copy-done.4
  79.3 0.0 copy-done.6
  79.3 3.7 %shard_map.144.proj_ref = f32[256,384]{1,0:T(8,128)S(1)} custom-call(bf16[32,8,4096]{2,1,0:T(8,128)(2,1)S(1)} %get-tuple-element.9.x_ref, f32[1,4096]{1,0:T(1,128)S(1)} %get-tuple-element.14.gain_ref, bf16[2,1,64,4096]{3,2,1,0:T(8,128)(2,1)S(1)} %bitcast.13, bf16[2,1,64,4096]{3,2,1,0:T(8,128)(2,1)S(1)} %bitcast.15, bf16[2,1,64,4096]{3,2,1,0:T(8,128)(2,1)S(1)} %bitcast.17, ...), custom_call_target="tpu_custom_call" | custom-call | tf_op jit(solution)/shard_map/pallas_call | solution.py:476
  83.0 9.2 %shard_map.145 = (bf16[16,2,8,4096]{3,2,1,0:T(8,128)(2,1)S(1)}, f32[2,1,256,4096]{3,2,1,0:T(8,128)}) custom-call(f32[256,384]{1,0:T(8,128)S(1)} %shard_map.144.proj_ref, f32[2,1,256,4096]{3,2,1,0:T(8,128)} %state_ref.3, f32[3,64]{1,0:T(4,128)S(1)} %get-tuple-element.16.table_ref, ...), custom_call_target="tpu_custom_call", output_to_operand_aliasing={{1}: (5, {})} | custom-call | tf_op jit(solution)/shard_map/pallas_call | solution.py:565
  92.1 18.4 %shard_map.146 = bf16[8,4096]{1,0:T(8,128)(2,1)S(1)} custom-call(bf16[16,2,8,4096]{3,2,1,0:T(8,128)(2,1)S(1)} %get-tuple-element.11.part_ref, bf16[8,4096]{1,0:T(8,128)(2,1)S(1)} %get-tuple-element.12.own_ref), custom_call_target="tpu_custom_call" | custom-call | tf_op jit(solution)/shard_map/pallas_call | solution.py:417
  110.6 0.6 copy.18
  (3 shorter events, 0.0 us)
Async XLA Ops:
  0.6 26.4 %copy-start.2 = (bf16[2,1,4096,64]{2,3,1,0:T(8,128)(2,1)S(1)}, bf16[2,1,4096,64]{2,3,1,0:T(8,128)(2,1)}, u32[]{:S(2)}) copy-start(bf16[2,1,4096,64]{2,3,1,0:T(8,128)(2,1)} %param.17) | copy-start | bytes 3145732
  0.6 26.4 %copy-start.1 = (bf16[2,1,4096,64]{2,3,1,0:T(8,128)(2,1)S(1)}, bf16[2,1,4096,64]{2,3,1,0:T(8,128)(2,1)}, u32[]{:S(2)}) copy-start(bf16[2,1,4096,64]{2,3,1,0:T(8,128)(2,1)} %param.16) | copy-start | bytes 3145732
  0.7 26.4 %copy-start = (bf16[2,1,4096,64]{2,3,1,0:T(8,128)(2,1)S(1)}, bf16[2,1,4096,64]{2,3,1,0:T(8,128)(2,1)}, u32[]{:S(2)}) copy-start(bf16[2,1,4096,64]{2,3,1,0:T(8,128)(2,1)} %param.15) | copy-start | bytes 3145732
  4.3 0.8 copy-start.10
  27.1 1.2 %copy-start.3 = (bf16[2,1,4096,64]{2,3,1,0:T(8,128)(2,1)S(1)}, bf16[2,1,4096,64]{2,3,1,0:T(8,128)(2,1)}, u32[]{:S(2)}) copy-start(bf16[2,1,4096,64]{2,3,1,0:T(8,128)(2,1)} %param.18) | copy-start | bytes 3145732
  28.3 1.2 %copy-start.5 = (bf16[2,1,4096,64]{2,3,1,0:T(8,128)(2,1)S(1)}, bf16[2,1,4096,64]{2,3,1,0:T(8,128)(2,1)}, u32[]{:S(2)}) copy-start(bf16[2,1,4096,64]{2,3,1,0:T(8,128)(2,1)} %param.19) | copy-start | bytes 3145732
  29.5 1.2 %copy-start.7 = (bf16[2,1,4096,64]{2,3,1,0:T(8,128)(2,1)S(1)}, bf16[2,1,4096,64]{2,3,1,0:T(8,128)(2,1)}, u32[]{:S(2)}) copy-start(bf16[2,1,4096,64]{2,3,1,0:T(8,128)(2,1)} %param.20) | copy-start | bytes 3145732
  30.7 3.7 %copy-start.9 = (bf16[2,1,64,4096]{3,2,1,0:T(8,128)(2,1)S(1)}, bf16[2,1,64,4096]{3,2,1,0:T(8,128)(2,1)}, u32[]{:S(2)}) copy-start(bf16[2,1,64,4096]{3,2,1,0:T(8,128)(2,1)} %w_ref.3) | copy-start | bytes 3145732
  34.4 9.3 %copy-start.11 = (bf16[1,8,4096]{2,1,0:T(8,128)(2,1)S(1)}, bf16[1,8,4096]{2,1,0:T(8,128)(2,1)}, u32[]{:S(2)}) copy-start(bf16[1,8,4096]{2,1,0:T(8,128)(2,1)} %param.13) | copy-start | bytes 196612
  34.4 44.8 %copy-start.8 = (bf16[2,1,4096,64]{2,3,1,0:T(8,128)(2,1)S(1)}, bf16[2,1,4096,64]{2,3,1,0:T(8,128)(2,1)}, u32[]{:S(2)}) copy-start(bf16[2,1,4096,64]{2,3,1,0:T(8,128)(2,1)} %param.20) | copy-start | bytes 3145732
  43.7 35.6 %copy-start.4 = (bf16[2,1,4096,64]{2,3,1,0:T(8,128)(2,1)S(1)}, bf16[2,1,4096,64]{2,3,1,0:T(8,128)(2,1)}, u32[]{:S(2)}) copy-start(bf16[2,1,4096,64]{2,3,1,0:T(8,128)(2,1)} %param.18) | copy-start | bytes 3145732
  43.7 35.6 %copy-start.6 = (bf16[2,1,4096,64]{2,3,1,0:T(8,128)(2,1)S(1)}, bf16[2,1,4096,64]{2,3,1,0:T(8,128)(2,1)}, u32[]{:S(2)}) copy-start(bf16[2,1,4096,64]{2,3,1,0:T(8,128)(2,1)} %param.19) | copy-start | bytes 3145732

commit v3 on v2

--- a/solution.py
+++ b/solution.py
@@ -310,10 +310,49 @@
         copy.wait_send()
 
 
-def gather_kernel(n, own_ref, full_ref, send, recv_a, recv_b):
+def start_loads(layer, weights, joined_ref, load):
+    head = weights[0].shape[2]
+    loads = [
+        pltpu.make_async_copy(w.at[layer, 0], joined_ref.at[pl.ds(i * head, head)], load.at[i])
+        for i, w in enumerate(weights)
+    ]
+    for copy in loads:
+        copy.start()
+    return loads
+
+
+def project_rows(layer, x_ref, gain_ref, w_ref, out_ref):
+    columns = x_ref.shape[2]
+    chunk = columns // 8
+    acc, squares = None, None
+    for at in range(0, columns, chunk):
+        wide = x_ref[:, :, at : at + chunk].astype(jnp.float32).reshape(-1, chunk)
+        scaled = (wide * gain_ref[layer : layer + 1, at : at + chunk]).astype(jnp.bfloat16)
+        part = lax.dot_general(
+            scaled,
+            w_ref[:, at : at + chunk],
+            (((1,), (1,)), ((), ())),
+            preferred_element_type=jnp.float32,
+        )
+        square = wide * wide
+        folded = square[:, :128]
+        for lane in range(128, chunk, 128):
+            folded = folded + square[:, lane : lane + 128]
+        acc = part if acc is None else acc + part
+        squares = folded if squares is None else squares + folded
+    mean = jnp.sum(squares, axis=1, keepdims=True) / columns
+    out_ref[...] = acc * lax.rsqrt(mean + RMS_EPS)
+
+
+def gather_kernel(n, own_ref, gain_ref, *refs, layer):
+    weights, (proj_ref, full_ref, joined_ref, load, *sems) = refs[:6], refs[6:]
+    loads = start_loads(layer, weights, joined_ref, load)
     at = Place(n)
     at.greet()
-    gather_phase(at, own_ref, full_ref, send, recv_a, recv_b)
+    gather_phase(at, own_ref, full_ref, *sems)
+    for copy in loads:
+        copy.wait()
+    project_rows(layer, full_ref, gain_ref, joined_ref, proj_ref)
 
 
 def sum_scratch(n, rows, columns):
@@ -397,12 +436,17 @@
     return total
 
 
-def middle_kernel(n, part_ref, own_ref, full_ref, next_ref, *scratch):
+def middle_kernel(n, part_ref, own_ref, gain_ref, *refs, layer):
+    weights, (proj_ref, next_ref, full_ref, joined_ref, load, *rest) = refs[:6], refs[6:]
+    loads = start_loads(layer, weights, joined_ref, load)
     at = Place(n)
     at.greet()
-    total = sum_phase(at, part_ref, scratch[:10])
+    total = sum_phase(at, part_ref, rest[3:])
     next_ref[...] = (own_ref[...].astype(jnp.float32) + total).astype(jnp.bfloat16)
-    gather_phase(at, next_ref, full_ref, *scratch[10:])
+    gather_phase(at, next_ref, full_ref, *rest[:3])
+    for copy in loads:
+        copy.wait()
+    project_rows(layer, full_ref, gain_ref, joined_ref, proj_ref)
 
 
 def last_kernel(n, part_ref, own_ref, next_ref, *scratch):
@@ -413,16 +457,17 @@
 
 
 def comm_call(kernel, n, collective_id, out_shape, scratch_shapes, *operands):
-    vmem = pl.BlockSpec(memory_space=pltpu.VMEM)
+    vmem, hbm = [pl.BlockSpec(memory_space=m) for m in (pltpu.VMEM, pltpu.HBM)]
     return pl.pallas_call(
         functools.partial(kernel, n),
         out_shape=out_shape,
-        in_specs=[vmem] * len(operands),
+        in_specs=[hbm if o.ndim == 4 and o.shape[0] != n // 2 else vmem for o in operands],
         out_specs=jax.tree.map(lambda _: vmem, out_shape),
         scratch_shapes=scratch_shapes,
         compiler_params=pltpu.CompilerParams(
-            collective_id=collective_id, has_side_effects=True, vmem_limit_bytes=40 << 20
+            collective_id=collective_id, has_side_effects=True, vmem_limit_bytes=(14 if collective_id == 2 else 58) << 20
         ),
+        cost_estimate=pl.CostEstimate(flops=0, bytes_accessed=50 << 20, transcendentals=0),
     )(*operands)
 
 
@@ -438,66 +483,23 @@
     return jnp.concatenate([v] * times, axis=1)
 
 
-def project_kernel(x_ref, gain_ref, *refs):
-    weights, (out_ref, acc, squares) = refs[:6], refs[6:]
-    step, last = pl.program_id(0), pl.num_programs(0) - 1
-    width = x_ref.shape[2]
-    wide = x_ref[...].astype(jnp.float32).reshape(-1, width)
-    scaled = (wide * gain_ref[...]).astype(jnp.bfloat16)
-    joined = jnp.concatenate([w[0, 0] for w in weights], axis=0)
-    part = lax.dot_general(
-        scaled, joined, (((1,), (1,)), ((), ())), preferred_element_type=jnp.float32
-    )
-    square = wide * wide
-    folded = square[:, :128]
-    for at in range(128, width, 128):
-        folded = folded + square[:, at : at + 128]
-
-    @pl.when(step == 0)
-    def _():
-        acc[...] = part
-        squares[...] = folded
-
-    @pl.when(step > 0)
-    def _():
-        acc[...] += part
-        squares[...] += folded
-
-    @pl.when(step == last)
-    def _():
-        mean = jnp.sum(squares[...], axis=1, keepdims=True) / (width * (last + 1))
-        out_ref[...] = acc[...] * lax.rsqrt(mean + RMS_EPS)
-
-
-def project(full, gain, weights, layer):
-    n, rows, columns = full.shape
-    head = weights[0].shape[2]
-    chunk = columns // 8
-    return pl.pallas_call(
-        project_kernel,
-        grid=(columns // chunk,),
-        in_specs=[
-            pl.BlockSpec((n, rows, chunk), lambda i: (0, 0, i)),
-            pl.BlockSpec((1, chunk), lambda i: (0, i)),
-        ]
-        + [pl.BlockSpec((1, 1, head, chunk), lambda i: (layer, 0, 0, i))] * 6,
-        out_specs=pl.BlockSpec((n * rows, 6 * head), lambda i: (0, 0)),
-        out_shape=jax.ShapeDtypeStruct((n * rows, 6 * head), jnp.float32),
-        scratch_shapes=[
-            pltpu.VMEM((n * rows, 6 * head), jnp.float32),
-            pltpu.VMEM((n * rows, 128), jnp.float32),
-        ],
-        compiler_params=pltpu.CompilerParams(vmem_limit_bytes=32 << 20),
-    )(full, gain[layer][None], *weights)
-
-
-def state_kernel(proj_ref, state_ref, table_ref, w_ref, spread_ref, *refs):
+def own_head(ref, layer, head):
+    position = lax.axis_index("tp")
+    start = pl.multiple_of(position // 2 * (2 * head), 2 * head)
+    pair = ref[layer : layer + 1, pl.ds(start, 2 * head)]
+    return jnp.where(position % 2 == 0, pair[:, :head], pair[:, head:])
+
+
+def state_kernel(
+    layer, proj_ref, state_ref, bias_ref, self_ref, gain_ref, w_ref, spread_ref, *refs
+):
     part_ref, new_ref = refs[-2:]
-    head = table_ref.shape[1]
+    head = w_ref.shape[2]
+    bias, self_w, ro_gain = [own_head(t, layer, head) for t in (bias_ref, self_ref, gain_ref)]
     rows, flat = state_ref.shape[2:]
     chunk = 8 * head
     r, k, v, p, q, g = [proj_ref[:, i * head : (i + 1) * head] for i in range(6)]
-    decay = jnp.exp(-jax.nn.sigmoid(table_ref[0:1] + p) * jnp.exp(jnp.float32(-0.5)))
+    decay = jnp.exp(-jax.nn.sigmoid(bias + p) * jnp.exp(jnp.float32(-0.5)))
     rate = jax.nn.sigmoid(q)
     kn = k * lax.rsqrt(jnp.sum(k * k, axis=1, keepdims=True) + 1.0)
     taken, added = kn * rate, k * rate
@@ -521,8 +523,8 @@
     center = jnp.mean(read, axis=1, keepdims=True)
     off = read - center
     spread = jnp.mean(off * off, axis=1, keepdims=True)
-    normed = off * lax.rsqrt(spread + GROUP_EPS) * table_ref[2:3]
-    own_term = jnp.sum(r * k * table_ref[1:2], axis=1, keepdims=True) * v
+    normed = off * lax.rsqrt(spread + GROUP_EPS) * ro_gain
+    own_term = jnp.sum(r * k * self_w, axis=1, keepdims=True) * v
     o = ((normed + own_term) * jax.nn.sigmoid(g)).astype(jnp.bfloat16)
 
     pair = jnp.concatenate([removed, v], axis=0)
@@ -544,17 +546,17 @@
         )
 
 
-def state_step(n, tile_rows, proj, state, table, w_out, spread, layer, earlier):
+def state_step(n, tile_rows, proj, state, tables, w_out, spread, layer, earlier):
     seqs, flat = state.shape[2:]
     head, columns = w_out.shape[2:]
     rows = seqs // 2
     state_spec = pl.BlockSpec((1, 1, rows, flat), lambda i: (layer, 0, i, 0))
     whole = lambda a: pl.BlockSpec(a.shape, lambda i: (0,) * a.ndim)
-    operands = [proj, state, table, w_out, spread]
+    operands = [proj, state, *tables, w_out, spread]
     in_specs = [
         pl.BlockSpec((rows, proj.shape[1]), lambda i: (i, 0)),
         state_spec,
-        whole(table),
+        *[whole(t) for t in tables],
         pl.BlockSpec((1, 1, head, columns), lambda i: (layer, 0, 0, 0)),
         whole(spread),
     ]
@@ -563,7 +565,7 @@
         in_specs.append(pl.BlockSpec(memory_space=pl.ANY))
     per = rows // tile_rows // 2
     return pl.pallas_call(
-        state_kernel,
+        functools.partial(state_kernel, layer),
         grid=(2,),
         in_specs=in_specs,
         out_specs=(
@@ -574,7 +576,7 @@
             jax.ShapeDtypeStruct((n // 2, 2, tile_rows, columns), jnp.bfloat16),
             jax.ShapeDtypeStruct(state.shape, jnp.float32),
         ),
-        input_output_aliases={} if earlier is None else {5: 1},
+        input_output_aliases={} if earlier is None else {7: 1},
         compiler_params=pltpu.CompilerParams(vmem_limit_bytes=48 << 20),
     )(*operands)
 
@@ -586,39 +588,42 @@
     rows, columns = own.shape
     head = wr.shape[3]
     flat = state.shape[3]
-    full_shape = jax.ShapeDtypeStruct((n, rows, columns), own.dtype)
+    proj_shape = jax.ShapeDtypeStruct((n * rows, 6 * head), jnp.float32)
+    gather_space = [
+        pltpu.VMEM((n, rows, columns), own.dtype),
+        pltpu.VMEM((6 * head, columns), wr.dtype),
+        pltpu.SemaphoreType.DMA((6,)),
+    ] + gather_scratch(n)
     own_shape = jax.ShapeDtypeStruct(own.shape, own.dtype)
-    position = lax.axis_index("tp")
-    tables = jnp.stack([bias, self_w, ro_gain], axis=1)
-    tables = lax.dynamic_slice_in_dim(tables, position * head, head, 2)
+    tables = (bias, self_w, ro_gain)
     value_of = jnp.arange(flat) // head
     spread = (jnp.arange(2 * head)[:, None] % head == value_of[None]).astype(jnp.bfloat16)
 
-    def mixer(full, layer, earlier):
-        proj = project(full, gain, weights, layer)
-        return state_step(
-            n, rows, proj, state, tables[layer], w_out, spread, layer, earlier
-        )
-
-    full = comm_call(gather_kernel, n, 0, full_shape, gather_scratch(n), own)
-    part, new_state = mixer(full, 0, None)
-    full, own = comm_call(
-        middle_kernel,
+    def mixer(proj, layer, earlier):
+        return state_step(n, rows, proj, state, tables, w_out, spread, layer, earlier)
+
+    first = functools.partial(gather_kernel, layer=0)
+    proj = comm_call(first, n, 0, proj_shape, gather_space, own, gain, *weights)
+    part, new_state = mixer(proj, 0, None)
+    proj, own = comm_call(
+        functools.partial(middle_kernel, layer=1),
         n,
         1,
-        (full_shape, own_shape),
-        sum_scratch(n, rows, columns) + gather_scratch(n),
+        (proj_shape, own_shape),
+        gather_space + sum_scratch(n, rows, columns),
         part,
         own,
-    )
-    part, new_state = mixer(full, 1, new_state)
+        gain,
+        *weights,
+    )
+    part, new_state = mixer(proj, 1, new_state)
     mixed = comm_call(last_kernel, n, 2, own_shape, sum_scratch(n, rows, columns), part, own)
     return mixed[None], new_state
 
 
 def pick(n, *args):
     one_block = args[0].shape[2] == args[1].shape[1]
-    if one_block and n % 16 == 0:
+    if one_block and n % 16 == 0 and 2 * args[2].shape[3] % 128 == 0:
         return on_device_fast(n, *args)
     return on_device(*args)
 

time: 112 us -> 106 us (0.946)
  local copies, waits for them, and re-layouts: 8.42 us -> 3.97 us
    pallas_call x4 -> x2, Pallas kernels: 25.7 us -> 18.6 us  [state_step(): pl.pallas_call(functools.partial(state_kernel, layer), grid=(2,), in_spec...]
    pallas_call x3, Pallas kernels: 75.9 us -> 82.7 us  [comm_call(): pl.pallas_call(functools.partial(kernel, n), out_shape=out_shape, in_spec...]
    another operation x3 -> x0, local copies, waits for them, and re-layouts: 2.37 us -> none  [on_device_fast(): tables = jnp.stack([bias, self_w, ro_gain], axis=1)]
    unnamed x25 -> x17, local copies, waits for them, and re-layouts: 5.17 us -> 3.97 us
where the time goes in v3:
time: 106 us
  Pallas kernels  101 us (95%)
  local copies, waits for them, and re-layouts  3.97 us (4%)
    pallas_call x3, Pallas kernels, comm_call(): pl.pallas_call(functools.partial(kernel, n), out_shape=out_shape, in_spec...  82.7 us
    pallas_call x2, Pallas kernels, state_step(): pl.pallas_call(functools.partial(state_kernel, layer), grid=(2,), in_spec...  18.6 us
    unnamed x17, local copies, waits for them, and re-layouts  3.97 us

profile of v3, /device:TPU:0, one launch (start us, length us, event | category | flops | bytes accessed | tf_op | source)
XLA Modules:
  0.0 106.2 jit_solution(4499699834130908464)
XLA Ops:
  0.7 0.0 copy-start
  0.7 0.0 copy-start.5
  0.7 0.0 copy-start.6
  0.7 0.0 copy-start.7
  0.7 25.0 %shard_map.140.proj_ref = f32[256,384]{1,0:T(8,128)} custom-call(bf16[8,4096]{1,0:T(8,128)(2,1)} %bitcast.21, f32[2,4096]{1,0:T(2,128)} %gain_ref.6, bf16[2,1,64,4096]{3,2,1,0:T(8,128)(2,1)} %bitcast.9, bf16[2,1,64,4096]{3,2,1,0:T(8,128)(2,1)} %bitcast.11, bf16[2,1,64,4096]{3,2,1,0:T(8,128)(2,1)} %bitcast.13, bf16[2,1,64,4096]{3,2,1,0:T(8,128)(2,1)} %bitcast.15, ...), custom_call_target="tpu_custom_call" | custom-call | bytes 52428800 | tf_op jit(solution)/shard_map/pallas_call | solution.py:461
  25.7 0.3 compare_convert_fusion.spread_ref
  25.9 0.0 copy-done
  25.9 0.0 copy-done.5
  26.0 0.0 copy-done.6
  26.0 0.0 copy-done.7
  26.0 0.0 copy-start.2
  26.0 1.0 copy-done.2
  27.0 9.3 %shard_map.141 = (bf16[16,2,8,4096]{3,2,1,0:T(8,128)(2,1)S(1)}, f32[2,1,256,4096]{3,2,1,0:T(8,128)}) custom-call(f32[256,384]{1,0:T(8,128)S(1)} %copy-done.2, f32[2,1,256,4096]{3,2,1,0:T(8,128)} %state_ref.3, f32[2,2048]{1,0:T(2,128)S(1)} %copy-done.5, f32[2,2048]{1,0:T(2,128)S(1)} %copy-done.6, f32[2,2048]{1,0:T(2,128)S(1)} %copy-done.7, ...), custom_call_target="tpu_custom_call" | custom-call | tf_op jit(solution)/shard_map/pallas_call | solution.py:567
  36.2 0.0 copy-start.1
  36.2 1.3 %copy-done.1 = bf16[16,2,8,4096]{3,2,1,0:T(8,128)(2,1)} copy-done((bf16[16,2,8,4096]{3,2,1,0:T(8,128)(2,1)}, bf16[16,2,8,4096]{3,2,1,0:T(8,128)(2,1)S(1)}, u32[]{:S(2)}) %copy-start.1) | copy-done | bytes 2097176
  37.6 39.3 %shard_map.142 = (f32[256,384]{1,0:T(8,128)}, bf16[8,4096]{1,0:T(8,128)(2,1)}) custom-call(bf16[16,2,8,4096]{3,2,1,0:T(8,128)(2,1)} %copy-done.1, bf16[8,4096]{1,0:T(8,128)(2,1)} %bitcast.22, f32[2,4096]{1,0:T(2,128)} %gain_ref.6, bf16[2,1,64,4096]{3,2,1,0:T(8,128)(2,1)} %bitcast.10, bf16[2,1,64,4096]{3,2,1,0:T(8,128)(2,1)} %bitcast.12, ...), custom_call_target="tpu_custom_call" | custom-call | bytes 52428800 | tf_op jit(solution)/shard_map/pallas_call | solution.py:461
  76.8 0.0 copy-start.3
  76.9 1.0 copy-done.3
  77.8 0.0 copy-start.4
  77.8 9.3 %shard_map.143 = (bf16[16,2,8,4096]{3,2,1,0:T(8,128)(2,1)S(1)}, f32[2,1,256,4096]{3,2,1,0:T(8,128)}) custom-call(f32[256,384]{1,0:T(8,128)S(1)} %copy-done.3, f32[2,1,256,4096]{3,2,1,0:T(8,128)} %state_ref.3, f32[2,2048]{1,0:T(2,128)S(1)} %copy-done.5, f32[2,2048]{1,0:T(2,128)S(1)} %copy-done.6, ...), custom_call_target="tpu_custom_call", output_to_operand_aliasing={{1}: (7, {})} | custom-call | tf_op jit(solution)/shard_map/pallas_call | solution.py:567
  87.2 0.0 copy-done.4
  87.2 18.4 %shard_map.144 = bf16[8,4096]{1,0:T(8,128)(2,1)S(1)} custom-call(bf16[16,2,8,4096]{3,2,1,0:T(8,128)(2,1)S(1)} %get-tuple-element.11.part_ref, bf16[8,4096]{1,0:T(8,128)(2,1)S(1)} %copy-done.4), custom_call_target="tpu_custom_call" | custom-call | bytes 52428800 | tf_op jit(solution)/shard_map/pallas_call | solution.py:461
  105.6 0.6 copy.18
  (2 shorter events, 0.0 us)
Async XLA Ops:
  0.7 25.3 %copy-start = (bf16[2,1,64,4096]{3,2,1,0:T(8,128)(2,1)S(1)}, bf16[2,1,64,4096]{3,2,1,0:T(8,128)(2,1)}, u32[]{:S(2)}) copy-start(bf16[2,1,64,4096]{3,2,1,0:T(8,128)(2,1)} %w_ref.3) | copy-start | bytes 3145732
  0.7 25.3 %copy-start.5 = (f32[2,2048]{1,0:T(2,128)S(1)}, f32[2,2048]{1,0:T(2,128)}, u32[]{:S(2)}) copy-start(f32[2,2048]{1,0:T(2,128)} %bias_ref.3) | copy-start | bytes 49156
  0.7 25.3 %copy-start.6 = (f32[2,2048]{1,0:T(2,128)S(1)}, f32[2,2048]{1,0:T(2,128)}, u32[]{:S(2)}) copy-start(f32[2,2048]{1,0:T(2,128)} %self_ref.3) | copy-start | bytes 49156
  0.7 25.3 %copy-start.7 = (f32[2,2048]{1,0:T(2,128)S(1)}, f32[2,2048]{1,0:T(2,128)}, u32[]{:S(2)}) copy-start(f32[2,2048]{1,0:T(2,128)} %gain_ref.7) | copy-start | bytes 49156
  26.0 1.0 copy-start.2
  36.2 1.3 %copy-start.1 = (bf16[16,2,8,4096]{3,2,1,0:T(8,128)(2,1)}, bf16[16,2,8,4096]{3,2,1,0:T(8,128)(2,1)S(1)}, u32[]{:S(2)}) copy-start(bf16[16,2,8,4096]{3,2,1,0:T(8,128)(2,1)S(1)} %get-tuple-element.8.part_ref) | copy-start | bytes 6291460
  76.8 1.0 copy-start.3
  77.8 9.3 %copy-start.4 = (bf16[8,4096]{1,0:T(8,128)(2,1)S(1)}, bf16[8,4096]{1,0:T(8,128)(2,1)}, u32[]{:S(2)}) copy-start(bf16[8,4096]{1,0:T(8,128)(2,1)} %get-tuple-element.12.own_ref) | copy-start | bytes 196612
